TPU v7x, 32 devices: a whole 2x2x4 slice. The times are simulated.
32 devices in a mesh: ep: 8 (over z, y), tp: 4 (over x, core).
Axes of the slice: x: 2, y: 2, z: 4, core: 2. Of those that a mesh axis runs over, the one named last changes fastest.
Arguments:
- queries: bfloat16 [16384, 1024], P('ep', 'tp'), may hold values from -6 to 6
- keys_values: bfloat16 [16384, 512], P('ep', 'tp'), may hold values from -6 to 6
- sink_logits: float32 [16], replicated, may hold values from 4 to 8
- out_weight: bfloat16 [1024, 2048], replicated, may hold values from -4 to 4
- expert_tokens: bfloat16 [8192, 2048], P(('ep', 'tp')), may hold values from -6 to 6
- norm_gain: float32 [2048], replicated, may hold values from 0.1 to 1.9
- routes: int32 [8192, 2], P(('ep', 'tp')), may hold values from 0 to 7, all different within a row; in each aligned block of 256 rows (0 to 255, 256 to 511, ...) at most 96 rows name the same one
- route_weights: float32 [8192, 2], P(('ep', 'tp')), may hold values from 0.1 to 1
- gate_weight: bfloat16 [8, 2048, 1024], P('ep', None, 'tp'), may hold values from -0.125 to 0.125
- up_weight: bfloat16 [8, 2048, 1024], P('ep', None, 'tp'), may hold values from -0.125 to 0.125
- down_weight: bfloat16 [8, 1024, 2048], P('ep', 'tp'), may hold values from -0.1875 to 0.1875
Outputs:
- mixer_out: bfloat16 [16384, 2048], P(('ep', 'tp'))
- expert_out: bfloat16 [8192, 2048], P(('ep', 'tp'))
Inputs may be any that keep to these rules, and one draw needn't show every extreme that they name: `routes`: each row names 2 different experts. In each aligned block of 256 rows, no expert is named by more than 96 rows, and in some block an expert is named by exactly 96 rows.
All inputs are finite; a program needn't handle non-finite values.
Results may differ from a plain program's by a relative error of at most 0.012.
Values may be sent and summed in bfloat16 or wider, within the bound.
No kernel may reach another device: no remote copies, remote signals or barrier semaphores. Data moves between devices by JAX's collectives and lax.ppermute only.
A program may use at most 128 MiB of HBM per device.

v0:
```python
import jax
import jax.numpy as jnp
from jax import lax
from jax.sharding import PartitionSpec as P

HEAD_DIM = 64
WINDOW = 128
TOPK = 2


NEG_FILL = -1e30


def padded_2(cells, sides, width):
    for axis, dim in sides:
        count = lax.axis_size(axis)
        ends = count - 1
        head = lax.slice_in_dim(cells, 0, width, axis=dim)
        tail = lax.slice_in_dim(cells, cells.shape[dim] - width, cells.shape[dim], axis=dim)
        cells = jnp.concatenate(
            [
                lax.ppermute(tail, axis, [(i, (i + 1) % count) for i in range(ends)]),
                cells,
                lax.ppermute(head, axis, [((i + 1) % count, i) for i in range(ends)]),
            ],
            axis=dim,
        )
    return cells


def widen_rows(token_rows, gate_local, up_local):
    gate_value = jnp.einsum(
        "etcd,df->etcf", token_rows, gate_local, preferred_element_type=jnp.float32
    )
    up_value = jnp.einsum("etcd,df->etcf", token_rows, up_local, preferred_element_type=jnp.float32)
    return (jax.nn.silu(gate_value) * up_value).astype(jnp.bfloat16)


def attend(queries, keys_values, sink_logits):
    row_count = queries.shape[0]
    kv_local = keys_values.shape[1] // (2 * HEAD_DIM)
    group_size = queries.shape[1] // (kv_local * HEAD_DIM)
    block_rows = min(512, row_count)
    key_span = block_rows + 2 * WINDOW
    padded = padded_2(keys_values, (("ep", 0),), WINDOW)
    offset = lax.axis_index("ep") * row_count
    seq_total = row_count * lax.axis_size("ep")
    head_first = lax.axis_index("tp") * (kv_local * group_size)
    sink_local = lax.dynamic_slice_in_dim(
        sink_logits, head_first, kv_local * group_size, 0
    ).reshape(kv_local, group_size, 1, 1)
    score_scale = HEAD_DIM ** (-0.5)

    def one_block(block_index):
        first_row = block_index * block_rows
        query_block = lax.dynamic_slice_in_dim(queries, first_row, block_rows, 0).reshape(
            block_rows, kv_local, group_size, HEAD_DIM
        )
        pair_block = lax.dynamic_slice_in_dim(padded, first_row, key_span, 0).reshape(
            key_span, kv_local, 2, HEAD_DIM
        )
        scores = (
            jnp.einsum(
                "qhgd,khd->hgqk",
                query_block,
                pair_block[:, :, 0],
                preferred_element_type=jnp.float32,
            )
            * score_scale
        )
        query_pos = offset + first_row + jnp.arange(block_rows, dtype=jnp.int32)
        key_pos = offset + first_row - WINDOW + jnp.arange(key_span, dtype=jnp.int32)
        allowed = (
            (jnp.abs(query_pos[:, None] - key_pos[None, :]) <= WINDOW)
            & (key_pos >= 0)[None, :]
            & (key_pos < seq_total)[None, :]
        )
        scores = jnp.where(allowed, scores, NEG_FILL)
        top_score = jnp.maximum(jnp.max(scores, -1, keepdims=True), sink_local)
        exp_scores = jnp.exp(scores - top_score)
        denominator = jnp.sum(exp_scores, -1, keepdims=True) + jnp.exp(sink_local - top_score)
        attn_weights = (exp_scores / denominator).astype(jnp.bfloat16)
        head_values = jnp.einsum(
            "hgqk,khd->qhgd", attn_weights, pair_block[:, :, 1], preferred_element_type=jnp.float32
        )
        return head_values.astype(jnp.bfloat16).reshape(
            block_rows, kv_local * group_size * HEAD_DIM
        )

    blocks = lax.map(one_block, jnp.arange(row_count // block_rows, dtype=jnp.int32))
    return blocks.reshape(row_count, kv_local * group_size * HEAD_DIM)


def body(
    queries,
    keys_values,
    sink_logits,
    out_weight,
    expert_tokens,
    norm_gain,
    routes,
    route_weights,
    gate_weight,
    up_weight,
    down_weight,
):
    tp_count = lax.axis_size("tp")
    ep_count = lax.axis_size("ep")
    attended = attend(queries, keys_values, sink_logits)
    token_rows = lax.all_to_all(attended, "tp", split_axis=0, concat_axis=1, tiled=True)
    mixer_out = jnp.dot(token_rows, out_weight, preferred_element_type=jnp.float32).astype(
        jnp.bfloat16
    )
    row_count = expert_tokens.shape[0]
    model_width = expert_tokens.shape[1]
    capacity = 3 * row_count * TOPK // (2 * ep_count)
    rows_float = expert_tokens.astype(jnp.float32)
    centred = rows_float - jnp.mean(rows_float, -1, keepdims=True)
    normed = (
        centred * lax.rsqrt(jnp.mean(centred * centred, -1, keepdims=True) + 1e-06) * norm_gain
    ).astype(jnp.bfloat16)
    flat_routes = routes.reshape(-1)
    one_hot = (flat_routes[:, None] == jnp.arange(ep_count, dtype=jnp.int32)[None, :]).astype(
        jnp.int32
    )
    slot_rank = jnp.sum((jnp.cumsum(one_hot, 0) - 1) * one_hot, 1)
    slot_index = flat_routes * capacity + slot_rank
    copy_token = jnp.arange(row_count * TOPK, dtype=jnp.int32) // TOPK
    slot_token = (
        jnp.full((ep_count * capacity,), row_count, jnp.int32).at[slot_index].set(copy_token)
    )
    outgoing = jnp.take(normed, slot_token, axis=0, mode="fill", fill_value=0).reshape(
        ep_count, capacity, model_width
    )
    gate_local = gate_weight[0]
    up_local = up_weight[0]
    down_local = down_weight[0]
    gate_whole, up_whole, down_whole = (
        lax.all_gather(gate_local, "tp", axis=1, tiled=True),
        lax.all_gather(up_local, "tp", axis=1, tiled=True),
        lax.all_gather(down_local, "tp", axis=0, tiled=True),
    )
    arrived = lax.all_to_all(outgoing, "ep", split_axis=0, concat_axis=0, tiled=True)
    hidden = widen_rows(arrived[:, None], gate_whole, up_whole)
    block_width = down_local.shape[0]
    hidden_blocks = hidden.reshape(ep_count * capacity, tp_count, block_width)
    down_blocks = down_whole.reshape(tp_count, block_width, model_width)
    partial_value = jnp.einsum(
        "rqf,qfd->qrd", hidden_blocks, down_blocks, preferred_element_type=jnp.float32
    ).astype(jnp.bfloat16)
    expert_rows = jnp.sum(partial_value.astype(jnp.float32), 0).astype(jnp.bfloat16)
    returned = lax.all_to_all(
        expert_rows.reshape(ep_count, capacity, model_width),
        "ep",
        split_axis=0,
        concat_axis=0,
        tiled=True,
    )
    per_copy = jnp.take(returned.reshape(ep_count * capacity, model_width), slot_index, axis=0)
    weighted = (
        per_copy.astype(jnp.float32).reshape(row_count, TOPK, model_width)
        * route_weights[:, :, None]
    )
    expert_out = jnp.sum(weighted, 1).astype(jnp.bfloat16)
    return (mixer_out, expert_out)


def solution(mesh):
    return jax.shard_map(
        body,
        mesh=mesh,
        in_specs=(
            P("ep", "tp"),
            P("ep", "tp"),
            P(),
            P(),
            P(("ep", "tp"), None),
            P(),
            P(("ep", "tp"), None),
            P(("ep", "tp"), None),
            P("ep", None, "tp"),
            P("ep", None, "tp"),
            P("ep", "tp", None),
        ),
        out_specs=(P(("ep", "tp"), None), P(("ep", "tp"), None)),
        check_vma=False,
    )
```

profile of v0, /device:TPU:0, one launch (start us, length us, event | category | flops | bytes accessed | tf_op | source)
XLA Modules:
  0.0 264.6 jit_solution(13465591957161986532)
XLA Ops:
  12.3 2.4 scatter_custom_fusion
  15.9 4.3 %gather_fusion = bf16[768,2048]{1,0:T(8,128)(2,1)} fusion(bf16[256,2048]{1,0:T(8,128)(2,1)S(1)} %fusion.24, s32[1024]{0:T(1024)S(1)} %pad_clamp_fusion.1), kind=kCustom, calls=%fused_computation | custom fusion | bytes 6294528 | tf_op jit(solution)/shard_map/jit(_take)/gather | solution.py:132
  20.3 4.2 %broadcast_select_fusion.1 = bf16[8,96,2048]{2,1,0:T(8,128)(2,1)} fusion(bf16[8,96,2048]{2,1,0:T(8,128)(2,1)} %bitcast.100, pred[8,96]{1,0:T(8,128)(4,1)S(1)} %broadcast_in_dim.67), kind=kLoop, calls=%fused_computation.36 | loop fusion | flops 1572864 | bytes 6292224 | tf_op jit(solution)/shard_map/jit(_take)/select_n | solution.py:132
  24.4 7.2 %all-to-all-start.1 = ((bf16[8,96,2048]{2,1,0:T(8,128)(2,1)}), bf16[8,96,2048]{2,1,0:T(8,128)(2,1)}, u32[]{:S(2)}, u32[]{:S(2)}) async-start(bf16[8,96,2048]{2,1,0:T(8,128)(2,1)} %broadcast_select_fusion.1), calls=%async_computation.1 | async-start | bytes 6291456 | tf_op jit(solution)/shard_map/all_to_all | solution.py:143
  31.9 3.9 %collective-permute-start = (bf16[128,128]{0,1:T(8,128)(2,1)S(1)}, bf16[128,128]{0,1:T(8,128)(2,1)S(1)}, u32[]{:S(2)}, u32[]{:S(2)}) collective-permute-start(bf16[128,128]{0,1:T(8,128)(2,1)S(1)} %get-tuple-element.131), channel_id=1, source_target_pairs={{0,4},{4,8},{8,12},{12,16},{16,20},{20,24},{24,28},{1,5},{5,9},{9,... | collective-permute-start | bytes 98312 | tf_op jit(solution)/shard_map/ppermute | solution.py:22
  37.2 21.0 %collective-permute-done = bf16[128,128]{0,1:T(8,128)(2,1)S(1)} collective-permute-done((bf16[128,128]{0,1:T(8,128)(2,1)S(1)}, bf16[128,128]{0,1:T(8,128)(2,1)S(1)}, u32[]{:S(2)}, u32[]{:S(2)}) %collective-permute-start) | collective-permute-done | bytes 32800 | tf_op jit(solution)/shard_map/ppermute | solution.py:22
  58.3 34.7 %while.12 = (s32[]{:T(128)}, bf16[4,512,256]{1,2,0:T(8,128)(2,1)}, s32[4]{0:T(128)S(1)}, bf16[2304,128]{0,1:T(8,128)(2,1)S(1)}, s32[]{:T(128)}, /*index=5*/bf16[...) while((s32[]{:T(128)}, bf16[4,512,256]{1,2,0:T(8,128)(2,1)}, ...), condition=%wide.region_3.4_spmd, body=%wide.region_0.3_spmd.sunk | while | flops 423632384 | bytes 23230236 | solution.py:90
  64.3 2.0 fusion.53
  73.0 2.0 fusion.53
  81.7 2.0 fusion.53
  88.9 1.4 fusion.52
  90.3 2.0 fusion.53
  93.1 9.7 %all-to-all-done.1 = bf16[8,96,2048]{2,1,0:T(8,128)(2,1)} async-done(((bf16[8,96,2048]{2,1,0:T(8,128)(2,1)}), bf16[8,96,2048]{2,1,0:T(8,128)(2,1)}, u32[]{:S(2)}, u32[]{:S(2)}) %all-to-all-start.1) | async-done | bytes 3145760 | tf_op jit(solution)/shard_map/all_to_all | solution.py:143
  102.8 4.4 %all-to-all-start = ((bf16[4,512,256]{1,2,0:T(8,128)(2,1)}), bf16[4,512,256]{1,2,0:T(8,128)(2,1)}, u32[]{:S(2)}, u32[]{:S(2)}) async-start(bf16[4,512,256]{1,2,0:T(8,128)(2,1)} %get-tuple-element.91), calls=%async_computation | async-start | bytes 2097152 | tf_op jit(solution)/shard_map/all_to_all | solution.py:110
  107.3 8.3 %fusion.14 = f32[8,96,1024]{2,1,0:T(8,128)} fusion(bf16[8,96,2048]{2,1,0:T(8,128)(2,1)} %all-to-all-done.1, bf16[1,2048,1024]{2,1,0:T(8,128)(2,1)} %all-gather.9.cloned.1.call-done), kind=kOutput, calls=%fused_computation.29 | convolution fusion | flops 3221225472 | bytes 10485760 | tf_op jit(solution)/shard_map/etcd,df->etcf/dot_general | solution.py:35
  115.5 7.9 %multiply_convert_fusion = bf16[8,96,1024]{2,1,0:T(8,128)(2,1)S(1)} fusion(f32[8,96,1024]{2,1,0:T(8,128)} %fusion.14, bf16[8,96,2048]{2,1,0:T(8,128)(2,1)} %all-to-all-done.1, bf16[1,2048,1024]{2,1,0:T(8,128)(2,1)} %all-gather.7.cloned.1.call-done), kind=kOutput, calls=%fused_computation.35 | convolution fusion | flops 3225944064 | bytes 12058624 | tf_op jit(solution)/shard_map/etcd,df->etcf/dot_general | solution.py:32
  124.6 3.5 %all-gather.11.cloned.1.call-done = bf16[1,1024,2048]{2,1,0:T(8,128)(2,1)} async-done(((bf16[1,256,2048]{2,1,0:T(8,128)(2,1)}), bf16[1,1024,2048]{2,1,0:T(8,128)(2,1)}) %all-gather.11.cloned.1.call-update) | async-done | bytes 4194320 | tf_op jit(solution)/shard_map/all_gather | solution.py:141
  128.2 8.5 %convert_reduce_fusion = bf16[768,2048]{1,0:T(8,128)(2,1)} fusion(bf16[4,256,2048]{2,1,0:T(8,128)(2,1)} %bitcast.110, bf16[768,4,256]{2,1,0:T(4,128)(2,1)S(1)} %reshape.283), kind=kOutput, calls=%fused_computation.28 | convolution fusion | flops 3232235520 | bytes 8912896 | tf_op jit(solution)/shard_map/rqf,qfd->qrd/dot_general | solution.py:148
  136.6 34.3 %all-to-all-start.2 = ((bf16[8,96,2048]{2,1,0:T(8,128)(2,1)}), bf16[8,96,2048]{2,1,0:T(8,128)(2,1)S(1)}, u32[]{:S(2)}, u32[]{:S(2)}) async-start(bf16[8,96,2048]{2,1,0:T(8,128)(2,1)} %bitcast.104), calls=%async_computation.2 | async-start | bytes 6291456 | tf_op jit(solution)/shard_map/all_to_all | solution.py:152
  171.5 6.2 %convolution_convert_fusion = bf16[512,2048]{1,0:T(8,128)(2,1)} fusion(bf16[512,1024]{0,1:T(8,128)(2,1)} %bitcast.16, bf16[1024,2048]{1,0:T(8,128)(2,1)} %param.16), kind=kOutput, calls=%fused_computation.37 | convolution fusion | flops 2148532224 | bytes 7340032 | tf_op jit(solution)/shard_map/dot_general | solution.py:111
  177.8 64.6 %all-to-all-done.2 = bf16[8,96,2048]{2,1,0:T(8,128)(2,1)S(1)} async-done(((bf16[8,96,2048]{2,1,0:T(8,128)(2,1)}), bf16[8,96,2048]{2,1,0:T(8,128)(2,1)S(1)}, u32[]{:S(2)}, u32[]{:S(2)}) %all-to-all-start.2) | async-done | bytes 3145760 | tf_op jit(solution)/shard_map/all_to_all | solution.py:152
  242.3 3.3 %gather_fusion.1 = bf16[512,2048]{1,0:T(8,128)(2,1)} fusion(bf16[768,2048]{1,0:T(8,128)(2,1)S(1)} %bitcast.98, s32[1024]{0:T(1024)S(1)} %pad_clamp_fusion), kind=kCustom, calls=%fused_computation.1 | custom fusion | bytes 4196352 | tf_op jit(solution)/shard_map/jit(_take)/gather | solution.py:159
  245.7 3.2 %gather.15 = bf16[256,2,2048]{2,1,0:T(2,128)(2,1)S(1)} reshape(bf16[512,2048]{1,0:T(8,128)(2,1)} %gather_fusion.1) | data formatting | bytes 4194304 | tf_op jit(solution)/shard_map/jit(_take)/gather | solution.py:159
  248.8 9.2 %multiply_reduce_fusion = bf16[256,2048]{1,0:T(8,128)(2,1)} fusion(bf16[256,2,2048]{2,1,0:T(2,128)(2,1)S(1)} %gather.15, pred[256,2]{1,0:T(8,128)(4,1)S(1)} %copy.39, f32[256,2]{1,0:T(8,128)S(1)} %copy.42), kind=kLoop, calls=%fused_computation.33 | loop fusion | flops 3670016 | bytes 3148288 | tf_op jit(solution)/shard_map/reduce_sum | solution.py:164
  (110 shorter events, 32.2 us)
Async XLA Ops:
  7.2 30.0 %copy-start = (f32[16]{0:T(128)S(1)}, f32[16]{0:T(128)}, u32[]{:S(2)}) copy-start(f32[16]{0:T(128)} %param.15) | copy-start | bytes 196
  7.2 7.7 %copy-start.1 = (bf16[256,2048]{1,0:T(8,128)(2,1)S(1)}, bf16[256,2048]{1,0:T(8,128)(2,1)}, u32[]{:S(2)}) copy-start(bf16[256,2048]{1,0:T(8,128)(2,1)} %param.17) | copy-start | bytes 3145732
  7.2 8.4 %copy-start.4 = (f32[2048]{0:T(1024)S(1)}, f32[2048]{0:T(1024)}, u32[]{:S(2)}) copy-start(f32[2048]{0:T(1024)} %param.18) | copy-start | bytes 24580
  7.2 100.1 %all-gather.9.cloned.1.call-start = ((), (), s32[]{:S(2)}) async-start(), calls=%async_computation.4 | async-start | bytes 5242880 | tf_op jit(solution)/shard_map/all_gather | solution.py:140
  7.9 107.6 %all-gather.7.cloned.1.call-start = ((), (), s32[]{:S(2)}) async-start(), calls=%async_computation.3 | async-start | bytes 5242880 | tf_op jit(solution)/shard_map/all_gather | solution.py:139
  24.4 7.2 %copy-start.2 = (bf16[2048,128]{1,0:T(8,128)(2,1)S(1)}, bf16[2048,128]{1,0:T(8,128)(2,1)}, u32[]{:S(2)}) copy-start(bf16[2048,128]{1,0:T(8,128)(2,1)} %param.14) | copy-start | bytes 1572868
  24.4 78.3 %all-to-all-start.1 = ((bf16[8,96,2048]{2,1,0:T(8,128)(2,1)}), bf16[8,96,2048]{2,1,0:T(8,128)(2,1)}, u32[]{:S(2)}, u32[]{:S(2)}) async-start(bf16[8,96,2048]{2,1,0:T(8,128)(2,1)} %broadcast_select_fusion.1), calls=%async_computation.1 | async-start | bytes 6291456 | tf_op jit(solution)/shard_map/all_to_all | solution.py:143
  31.6 96.5 %all-gather.11.cloned.1.call-start = ((), (), s32[]{:S(2)}) async-start(), calls=%async_computation.5 | async-start | bytes 5242880 | tf_op jit(solution)/shard_map/all_gather | solution.py:141
  31.9 26.3 %collective-permute-start = (bf16[128,128]{0,1:T(8,128)(2,1)S(1)}, bf16[128,128]{0,1:T(8,128)(2,1)S(1)}, u32[]{:S(2)}, u32[]{:S(2)}) collective-permute-start(bf16[128,128]{0,1:T(8,128)(2,1)S(1)} %get-tuple-element.131), channel_id=1, source_target_pairs={{0,4},{4,8},{8,12},{12,16},{16,20},{20,24},{24,28},{1,5},{5,9},{9,... | collective-permute-start | bytes 98312 | tf_op jit(solution)/shard_map/ppermute | solution.py:22
  35.8 22.4 %collective-permute-start.1 = (bf16[128,128]{0,1:T(8,128)(2,1)S(1)}, bf16[128,128]{0,1:T(8,128)(2,1)S(1)}, u32[]{:S(2)}, u32[]{:S(2)}) collective-permute-start(bf16[128,128]{0,1:T(8,128)(2,1)S(1)} %get-tuple-element.132), channel_id=1, source_target_pairs={{4,0},{8,4},{12,8},{16,12},{20,16},{24,20},{28,24},{5,1},{9,5},{13... | collective-permute-start | bytes 98312 | tf_op jit(solution)/shard_map/ppermute | solution.py:24
  102.8 33.8 %all-to-all-start = ((bf16[4,512,256]{1,2,0:T(8,128)(2,1)}), bf16[4,512,256]{1,2,0:T(8,128)(2,1)}, u32[]{:S(2)}, u32[]{:S(2)}) async-start(bf16[4,512,256]{1,2,0:T(8,128)(2,1)} %get-tuple-element.91), calls=%async_computation | async-start | bytes 2097152 | tf_op jit(solution)/shard_map/all_to_all | solution.py:110
  136.6 34.5 %copy-start.3 = (s32[256,2]{0,1:T(2,128)S(1)}, s32[256,2]{0,1:T(2,128)}, u32[]{:S(2)}) copy-start(s32[256,2]{0,1:T(2,128)} %param.19) | copy-start | bytes 6148
  136.6 34.7 %copy-start.5 = (f32[256,2]{0,1:T(2,128)S(1)}, f32[256,2]{0,1:T(2,128)}, u32[]{:S(2)}) copy-start(f32[256,2]{0,1:T(2,128)} %param.20) | copy-start | bytes 6148
  136.6 105.7 %all-to-all-start.2 = ((bf16[8,96,2048]{2,1,0:T(8,128)(2,1)}), bf16[8,96,2048]{2,1,0:T(8,128)(2,1)S(1)}, u32[]{:S(2)}, u32[]{:S(2)}) async-start(bf16[8,96,2048]{2,1,0:T(8,128)(2,1)} %bitcast.104), calls=%async_computation.2 | async-start | bytes 6291456 | tf_op jit(solution)/shard_map/all_to_all | solution.py:152
Sparse Core Ops, SparseCore 0:
  9.6 37.7 all-gather.8
  48.9 34.9 all-gather.6
  85.5 42.6 all-gather.10
where the time goes:
time: 265 us
  waiting for transfers between devices  100 us (38%)
  starting transfers between devices  51.2 us (19%)
  matrix products  43.6 us (16%)
  local copies, waits for them, and re-layouts  26.8 us (10%)
  other arithmetic  25.8 us (10%)
  between operations  14 us (5%)
  loops' own time  2.8 us (1%)
    all_to_all x1, waiting for transfers between devices, body(): lax.all_to_all(expert_rows.reshape(ep_count, capacity, model_width), 'ep'...  64.6 us
    all_to_all x1, starting transfers between devices, body(): lax.all_to_all(expert_rows.reshape(ep_count, capacity, model_width), 'ep'...  34.3 us
    ppermute x1, waiting for transfers between devices, padded_2(): lax.ppermute(tail, axis, [(i, (i + 1) % count) for i in range(ends)])  21 us
    all_to_all x1, waiting for transfers between devices, body(): lax.all_to_all(outgoing, 'ep', split_axis=0, concat_axis=0, tiled=True)  9.73 us
    reduce_sum x1, other arithmetic, body(): expert_out = jnp.sum(weighted, 1).astype(jnp.bfloat16)  9.22 us
    dot_general x1, matrix products, body(): jnp.einsum('rqf,qfd->qrd', hidden_blocks, down_blocks, preferred_element_...  8.49 us
    dot_general x1, matrix products, widen_rows(): jnp.einsum('etcd,df->etcf', token_rows, up_local, preferred_element_type=...  8.26 us
    dot_general x4, matrix products, one_block(): jnp.einsum('hgqk,khd->qhgd', attn_weights, pair_block[:, :, 1], preferred...  8.04 us
  transfers between devices with their start and end apart: 8, of which 4 were waited for; matrix products, arithmetic and copies ran while one was open for 30% of the time, Pallas kernels for 0%

commit v1 on v0

v1 whole, which is shorter than its diff:
```python
import math

import jax
import jax.numpy as jnp
from jax import lax
from jax.experimental import pallas as pl
from jax.experimental.pallas import tpu as pltpu
from jax.sharding import PartitionSpec as P


HEAD_DIM = 64
WINDOW = 128
TOPK = 2
CHUNKS = 2


NEG_FILL = -1e30


def padded_2(cells, sides, width):
    for axis, dim in sides:
        count = lax.axis_size(axis)
        ends = count - 1
        head = lax.slice_in_dim(cells, 0, width, axis=dim)
        tail = lax.slice_in_dim(cells, cells.shape[dim] - width, cells.shape[dim], axis=dim)
        cells = jnp.concatenate(
            [
                lax.ppermute(tail, axis, [(i, (i + 1) % count) for i in range(ends)]),
                cells,
                lax.ppermute(head, axis, [((i + 1) % count, i) for i in range(ends)]),
            ],
            axis=dim,
        )
    return cells


def gathered_parts(blocks, axis):
    count = lax.axis_size(axis)
    groups = {0: blocks}
    bit = count // 2
    while bit:
        pairs = [(i, i ^ bit) for i in range(count)]
        for held in sorted(groups):
            groups[held ^ bit] = tuple(lax.ppermute(block, axis, pairs) for block in groups[held])
        bit = bit // 2
    return [groups[held] for held in sorted(groups)]


def dispatch_kernel(tokens_ref, gain_ref, slots_ref, *out_refs):
    rows_float = tokens_ref[...].astype(jnp.float32)
    centred = rows_float - jnp.mean(rows_float, -1, keepdims=True)
    normed = (
        centred
        * lax.rsqrt(jnp.mean(centred * centred, -1, keepdims=True) + 1e-06)
        * gain_ref[...]
    ).astype(jnp.bfloat16)
    peers = slots_ref.shape[0]
    chunk = out_refs[0].shape[0]
    place = lax.broadcasted_iota(jnp.int32, (chunk, rows_float.shape[0]), 0)
    for number in range(len(out_refs) // peers):
        picks = [
            jnp.where(slots_ref[peer : peer + 1, :] == place + number * chunk, 1.0, 0.0)
            for peer in range(peers)
        ]
        chosen = jnp.dot(
            jnp.concatenate(picks, 0).astype(jnp.bfloat16),
            normed,
            preferred_element_type=jnp.float32,
        ).astype(jnp.bfloat16)
        for peer in range(peers):
            out_refs[number * peers + peer][...] = chosen[peer * chunk : (peer + 1) * chunk]


def dispatch(tokens, gain, slots, chunk, chunks):
    peers, row_count = slots.shape
    width = tokens.shape[1]
    sent = pl.pallas_call(
        dispatch_kernel,
        out_shape=[jax.ShapeDtypeStruct((chunk, width), jnp.bfloat16)] * (peers * chunks),
        cost_estimate=pl.CostEstimate(
            flops=2 * peers * chunks * chunk * row_count * width,
            bytes_accessed=2 * tokens.size + 2 * peers * chunks * chunk * width,
            transcendentals=row_count,
        ),
        name="dispatch",
    )(tokens, gain.reshape(1, width), slots)
    return [sent[number * peers : (number + 1) * peers] for number in range(chunks)]


def exchange(blocks, axis):
    count = lax.axis_size(axis)
    swapped = {
        k: lax.ppermute(blocks[k], axis, [(i, i ^ k) for i in range(count)])
        for k in range(count - 1, 0, -1)
    }
    return [blocks[0]] + [swapped[k] for k in range(1, count)]


def expert_kernel(*refs, peers, count):
    row_refs, sources, out_refs = refs[:peers], refs[peers : peers + count], refs[peers + count :]
    out_refs, held = out_refs[:peers], out_refs[peers:]
    rows_held, total_ref, arrivals = held[count:]
    row_copies = [
        pltpu.make_async_copy(source, rows_held.at[peer], arrivals.at[count + peer])
        for peer, source in enumerate(row_refs)
    ]
    copies = [
        pltpu.make_async_copy(source, place, arrivals.at[number])
        for number, (source, place) in enumerate(zip(sources, held))
    ]
    for copy in row_copies + copies:
        copy.start()
    for copy in row_copies:
        copy.wait()
    chunk, width = row_refs[0].shape
    rows = rows_held[...].reshape(peers * chunk, width)
    for number in range(0, count, 3):
        copies[number].wait()
        gate_value = jnp.dot(rows, held[number][...], preferred_element_type=jnp.float32)
        copies[number + 1].wait()
        up_value = jnp.dot(rows, held[number + 1][...], preferred_element_type=jnp.float32)
        hidden = (gate_value / (1.0 + jnp.exp(-gate_value)) * up_value).astype(jnp.bfloat16)
        copies[number + 2].wait()
        part = jnp.dot(hidden, held[number + 2][...], preferred_element_type=jnp.float32)
        if number + 3 < count:
            total_ref[...] = part if number == 0 else total_ref[...] + part
        else:
            total = (total_ref[...] + part if number else part).astype(jnp.bfloat16)
            for peer in range(peers):
                out_refs[peer][...] = total[peer * chunk : (peer + 1) * chunk]


def expert_chunk(blocks, parts):
    flat = [array for part in parts for array in part]
    peers = len(blocks)
    chunk, width = blocks[0].shape
    row_count = peers * chunk
    hidden_units = sum(part[0].shape[1] for part in parts)
    return pl.pallas_call(
        lambda *refs: expert_kernel(*refs, peers=peers, count=len(flat)),
        out_shape=[jax.ShapeDtypeStruct((chunk, width), jnp.bfloat16)] * peers,
        in_specs=[pl.BlockSpec(memory_space=pl.ANY)] * (peers + len(flat)),
        scratch_shapes=[pltpu.VMEM(array.shape, array.dtype) for array in flat]
        + [
            pltpu.VMEM((peers, chunk, width), jnp.bfloat16),
            pltpu.VMEM((row_count, width), jnp.float32),
            pltpu.SemaphoreType.DMA((len(flat) + peers,)),
        ],
        cost_estimate=pl.CostEstimate(
            flops=6 * row_count * width * hidden_units,
            bytes_accessed=sum(2 * array.size for array in flat) + 4 * row_count * width,
            transcendentals=row_count * hidden_units,
        ),
        name="expert",
    )(*blocks, *flat)


def combine_kernel(shares_ref, *refs, peers):
    block_refs, rest = refs[:peers], refs[peers:]
    out_ref, held, arrivals = rest[-3:]
    copies = [
        pltpu.make_async_copy(source, held.at[peer], arrivals.at[peer])
        for peer, source in enumerate(block_refs)
    ]
    for copy in copies:
        copy.start()
    for copy in copies:
        copy.wait()
    chunk, width = block_refs[0].shape
    both = jnp.dot(
        shares_ref[...],
        held[...].reshape(peers * chunk, width),
        preferred_element_type=jnp.float32,
    )
    row_count = out_ref.shape[0]
    total = both[:row_count] + both[row_count:]
    if len(rest) > 3:
        total = total + rest[0][...]
    out_ref[...] = total.astype(out_ref.dtype)


def combine(shares, blocks, earlier, kind):
    peers = len(blocks)
    chunk, width = blocks[0].shape
    row_count = shares.shape[0] // 2
    whole = pl.BlockSpec(memory_space=pltpu.VMEM)
    return pl.pallas_call(
        lambda *refs: combine_kernel(*refs, peers=peers),
        out_shape=jax.ShapeDtypeStruct((row_count, width), kind),
        in_specs=[whole] + [pl.BlockSpec(memory_space=pl.ANY)] * peers + [whole] * len(earlier),
        scratch_shapes=[
            pltpu.VMEM((peers, chunk, width), jnp.bfloat16),
            pltpu.SemaphoreType.DMA((peers,)),
        ],
        cost_estimate=pl.CostEstimate(
            flops=4 * row_count * peers * chunk * width,
            bytes_accessed=2 * peers * chunk * width + 6 * row_count * width,
            transcendentals=0,
        ),
        name="combine",
    )(shares, *blocks, *earlier)


def attend_kernel(limits_ref, sinks_ref, query_ref, pairs_ref, out_ref, *, group_size):
    block = pl.program_id(0)
    step = WINDOW
    span = step + 2 * WINDOW
    wide = 2 * HEAD_DIM
    scale = HEAD_DIM ** (-0.5) * math.log2(math.e)
    query_at = lax.broadcasted_iota(jnp.int32, (step, span), 0)
    key_at = lax.broadcasted_iota(jnp.int32, (step, span), 1)
    band = (key_at >= query_at) & (key_at <= query_at + 2 * WINDOW)
    low_half = lax.broadcasted_iota(jnp.int32, (span, wide), 1) < HEAD_DIM
    for part in range(query_ref.shape[0] // step):
        first = pl.multiple_of(block * query_ref.shape[0] + part * step, step)
        allowed = (
            band & (key_at >= limits_ref[0] - first) & (key_at < limits_ref[1] - first)
        )
        for kv_head in range(pairs_ref.shape[1] // wide):
            pair = pairs_ref[pl.ds(first, span), kv_head * wide : (kv_head + 1) * wide]
            turned = jnp.concatenate([pair[:, HEAD_DIM:], pair[:, :HEAD_DIM]], axis=1)
            zero = jnp.zeros_like(pair)
            keys = (jnp.where(low_half, pair, zero), jnp.where(low_half, zero, turned))
            values = (jnp.where(low_half, turned, zero), jnp.where(low_half, zero, pair))
            for two in range(group_size // 2):
                column = (kv_head * group_size + 2 * two) * HEAD_DIM
                query = query_ref[part * step : (part + 1) * step, column : column + wide]
                both = None
                for side in range(2):
                    sink = sinks_ref[kv_head * group_size + 2 * two + side]
                    scores = lax.dot_general(
                        query,
                        keys[side],
                        (((1,), (1,)), ((), ())),
                        preferred_element_type=jnp.float32,
                    )
                    scores = jnp.where(allowed, scores * scale, NEG_FILL)
                    top = jnp.maximum(jnp.max(scores, -1, keepdims=True), sink)
                    grown = jnp.exp2(scores - top)
                    denominator = jnp.sum(grown, -1, keepdims=True) + jnp.exp2(sink - top)
                    head = jnp.dot(
                        grown.astype(jnp.bfloat16),
                        values[side],
                        preferred_element_type=jnp.float32,
                    ) * (1.0 / denominator)
                    both = head if both is None else both + head
                out_ref[part * step : (part + 1) * step, column : column + wide] = both.astype(
                    out_ref.dtype
                )


def attend(queries, padded, sink_logits):
    row_count, width = queries.shape
    kv_local = padded.shape[1] // (2 * HEAD_DIM)
    group_size = width // (kv_local * HEAD_DIM)
    block_rows = min(2 * WINDOW, row_count)
    offset = lax.axis_index("ep") * row_count
    seq_total = row_count * lax.axis_size("ep")
    limits = jnp.stack([WINDOW - offset, seq_total + WINDOW - offset]).astype(jnp.int32)
    heads = kv_local * group_size
    sinks = lax.dynamic_slice_in_dim(sink_logits, lax.axis_index("tp") * heads, heads, 0)
    return pl.pallas_call(
        lambda *refs: attend_kernel(*refs, group_size=group_size),
        out_shape=jax.ShapeDtypeStruct(queries.shape, jnp.bfloat16),
        grid=(row_count // block_rows,),
        in_specs=[
            pl.BlockSpec(memory_space=pltpu.SMEM),
            pl.BlockSpec(memory_space=pltpu.SMEM),
            pl.BlockSpec((block_rows, width), lambda i: (i, 0)),
            pl.BlockSpec(padded.shape, lambda i: (0, 0)),
        ],
        out_specs=pl.BlockSpec((block_rows, width), lambda i: (i, 0)),
        cost_estimate=pl.CostEstimate(
            flops=24 * row_count * width * WINDOW,
            bytes_accessed=4 * queries.size + 2 * padded.size,
            transcendentals=3 * row_count * heads * WINDOW,
        ),
        name="attend",
    )(limits, sinks * math.log2(math.e), queries, padded)


def layer(
    queries,
    keys_values,
    sink_logits,
    out_weight,
    expert_tokens,
    norm_gain,
    routes,
    route_weights,
    gate_weight,
    up_weight,
    down_weight,
):
    ep_count = lax.axis_size("ep")
    padded = padded_2(keys_values, (("ep", 0),), WINDOW)
    weights = gathered_parts((gate_weight[0], up_weight[0], down_weight[0]), "tp")

    row_count = expert_tokens.shape[0]
    capacity = 3 * row_count * TOPK // (2 * ep_count)
    chunk = -(-capacity // (CHUNKS * 16)) * 16

    order = lax.axis_index("ep") ^ jnp.arange(ep_count, dtype=jnp.int32)
    named_each = routes[:, :, None] == order
    named = jnp.any(named_each, 1)
    copy_weight = jnp.sum(jnp.where(named_each, route_weights[:, :, None], 0.0), 1)
    places = jnp.arange(row_count, dtype=jnp.int32)
    earlier = (places[None, :] < places[:, None]).astype(jnp.bfloat16)
    rank = jnp.dot(earlier, named.astype(jnp.bfloat16), preferred_element_type=jnp.float32)
    slot = jnp.where(named, rank.astype(jnp.int32), -1)

    sent = dispatch(expert_tokens, norm_gain, slot.T, chunk, CHUNKS)
    arrived = []
    for number in range(CHUNKS):
        arrived.append(exchange(sent[number], "ep"))

    attended = attend(queries, padded, sink_logits)
    tp_count = lax.axis_size("tp")
    mine = lax.axis_index("tp")
    own_rows = attended.shape[0] // tp_count
    width = attended.shape[1]
    mixer_sum = None
    for other in range(tp_count):
        rows = lax.dynamic_slice_in_dim(attended, (mine ^ other) * own_rows, own_rows, 0)
        if other:
            rows = lax.ppermute(rows, "tp", [(i, i ^ other) for i in range(tp_count)])
        part = jnp.dot(
            rows,
            lax.dynamic_slice_in_dim(out_weight, (mine ^ other) * width, width, 0),
            preferred_element_type=jnp.float32,
        )
        mixer_sum = part if mixer_sum is None else mixer_sum + part
    mixer_out = mixer_sum.astype(jnp.bfloat16)

    gathered = ()
    for number in range(CHUNKS):
        results = expert_chunk(arrived[number], weights)
        returned = exchange(results, "ep")
        slots = number * chunk + jnp.arange(chunk, dtype=jnp.int32)
        share = jnp.where(
            slot[:, :, None] == slots[None, None, :], copy_weight[:, :, None], 0.0
        ).reshape(row_count, ep_count * chunk)
        share_high = lax.reduce_precision(share, 8, 7)
        shares = jnp.concatenate([share_high, share - share_high], 0).astype(jnp.bfloat16)
        last = number == CHUNKS - 1
        gathered = (
            combine(shares, returned, gathered, jnp.bfloat16 if last else jnp.float32),
        )
    return (mixer_out, gathered[0])


def solution(mesh):
    return jax.shard_map(
        layer,
        mesh=mesh,
        in_specs=(
            P("ep", "tp"),
            P("ep", "tp"),
            P(),
            P(),
            P(("ep", "tp"), None),
            P(),
            P(("ep", "tp"), None),
            P(("ep", "tp"), None),
            P("ep", None, "tp"),
            P("ep", None, "tp"),
            P("ep", "tp", None),
        ),
        out_specs=(P(("ep", "tp"), None), P(("ep", "tp"), None)),
        check_vma=False,
    )
```

time: 265 us -> 224 us (0.85)
  the two profiles are of different devices: /device:TPU:0 before, /device:TPU:9 now
where the time goes in v1:
time: 224 us
  starting transfers between devices  76.1 us (34%)
  Pallas kernels  61.2 us (27%)
  waiting for transfers between devices  56.7 us (25%)
  matrix products  15.8 us (7%)
  other arithmetic  6.35 us (3%)
  local copies, waits for them, and re-layouts  6.1 us (3%)
    ppermute x28, waiting for transfers between devices, exchange(): lax.ppermute(blocks[k], axis, [(i, i ^ k) for i in range(count)])  56.2 us
    ppermute x28, starting transfers between devices, exchange(): lax.ppermute(blocks[k], axis, [(i, i ^ k) for i in range(count)])  39.1 us
    pallas_call x2, Pallas kernels, expert_chunk(): pl.pallas_call(lambda *refs: expert_kernel(*refs, peers=peers, count=len(...  26.4 us
    ppermute x9, starting transfers between devices, gathered_parts(): lax.ppermute(block, axis, pairs)  21.1 us
    pallas_call x1, Pallas kernels, attend(): pl.pallas_call(lambda *refs: attend_kernel(*refs, group_size=group_size),...  20.4 us
    dot_general x4, matrix products, layer(): jnp.dot(rows, lax.dynamic_slice_in_dim(out_weight, (mine ^ other) * width...  15 us
    pallas_call x2, Pallas kernels, combine(): pl.pallas_call(lambda *refs: combine_kernel(*refs, peers=peers), out_shap...  10.5 us
    ppermute x3, starting transfers between devices, layer(): rows = lax.ppermute(rows, 'tp', [(i, i ^ other) for i in range(tp_count)])  9.81 us
  transfers between devices with their start and end apart: 42, of which 12 were waited for; matrix products, arithmetic and copies ran while one was open for 10% of the time, Pallas kernels for 23%

profile of v1, /device:TPU:9, one launch (start us, length us, event | category | flops | bytes accessed | tf_op | source)
XLA Modules:
  0.0 223.7 jit_solution(16427197374547821635)
XLA Ops:
  2.2 4.0 %dispatch.1 = (bf16[48,2048]{1,0:T(8,128)(2,1)}, bf16[48,2048]{1,0:T(8,128)(2,1)}, bf16[48,2048]{1,0:T(8,128)(2,1)}, bf16[48,2048]{1,0:T(8,128)(2,1)}, bf16[48,2...) custom-call(bf16[256,2048]{1,0:T(8,128)(2,1)} %tokens_ref.1, ...), custom_call_target="tpu_custom_call" | custom-call | flops 805306368 | bytes 4194304 | tf_op jit(solution)/shard_map/dispatch/pallas_call | solution.py:77
  10.3 4.2 %collective-permute-start.1 = (bf16[128,128]{1,0:T(8,128)(2,1)S(1)}, bf16[128,128]{1,0:T(8,128)(2,1)S(1)}, u32[]{:S(2)}, u32[]{:S(2)}) collective-permute-start(bf16[128,128]{1,0:T(8,128)(2,1)S(1)} %get-tuple-element.76), channel_id=1, source_target_pairs={{4,0},{8,4},{12,8},{16,12},{20,16},{24,20},{28,24},{5,1},{9,5},{13... | collective-permute-start | bytes 98312 | tf_op jit(solution)/shard_map/ppermute | solution.py:30
  21.9 3.6 %collective-permute-done.31.refs_4_ = bf16[48,2048]{1,0:T(8,128)(2,1)S(1)} collective-permute-done((bf16[48,2048]{1,0:T(8,128)(2,1)}, bf16[48,2048]{1,0:T(8,128)(2,1)S(1)}, u32[]{:S(2)}, u32[]{:S(2)}) %collective-permute-start.31) | collective-permute-done | bytes 196640 | tf_op jit(solution)/shard_map/ppermute | solution.py:93
  25.6 16.1 %collective-permute-start.12 = (bf16[2048,256]{1,0:T(8,128)(2,1)}, bf16[2048,256]{1,0:T(8,128)(2,1)}, u32[]{:S(2)}, u32[]{:S(2)}) collective-permute-start(bf16[2048,256]{1,0:T(8,128)(2,1)} %bitcast.17), channel_id=1, source_target_pairs={{0,1},{1,0},{2,3},{3,2},{4,5},{5,4},{6,7},{7,6},{8,9},{9,8},{10,11... | collective-permute-start | bytes 3145736 | tf_op jit(solution)/shard_map/ppermute | solution.py:44
  42.9 5.0 %collective-permute-done.33.refs_6_ = bf16[48,2048]{1,0:T(8,128)(2,1)S(1)} collective-permute-done((bf16[48,2048]{1,0:T(8,128)(2,1)}, bf16[48,2048]{1,0:T(8,128)(2,1)S(1)}, u32[]{:S(2)}, u32[]{:S(2)}) %collective-permute-start.33) | collective-permute-done | bytes 196640 | tf_op jit(solution)/shard_map/ppermute | solution.py:93
  51.4 5.8 %collective-permute-start.10 = (bf16[48,2048]{1,0:T(8,128)(2,1)}, bf16[48,2048]{1,0:T(8,128)(2,1)S(1)}, u32[]{:S(2)}, u32[]{:S(2)}) collective-permute-start(bf16[48,2048]{1,0:T(8,128)(2,1)} %get-tuple-element.40), channel_id=1, source_target_pairs={{0,24},{4,28},{8,16},{12,20},{16,8},{20,12},{24,0},{28,4},{1,25},{... | collective-permute-start | bytes 589832 | tf_op jit(solution)/shard_map/ppermute | solution.py:93
  59.1 3.3 %collective-permute-done.10.refs_6_ = bf16[48,2048]{1,0:T(8,128)(2,1)S(1)} collective-permute-done((bf16[48,2048]{1,0:T(8,128)(2,1)}, bf16[48,2048]{1,0:T(8,128)(2,1)S(1)}, u32[]{:S(2)}, u32[]{:S(2)}) %collective-permute-start.10) | collective-permute-done | bytes 196640 | tf_op jit(solution)/shard_map/ppermute | solution.py:93
  71.9 20.4 %attend.1 = bf16[2048,256]{1,0:T(8,128)(2,1)} custom-call(s32[2]{0:T(128)} %pad_add_fusion.refs_0_, f32[4]{0:T(128)} %dynamic-slice_multiply_fusion.refs_1_, bf16[2048,256]{1,0:T(8,128)(2,1)} %refs_2_.1, bf16[2304,128]{1,0:T(8,128)(2,1)} %pad_maximum_fusion.refs_3_), custom_call_target="tpu_custom_call" | custom-call | flops 1610612736 | bytes 2686976 | tf_op jit(solution)/shard_map/attend/pallas_call | solution.py:262
  94.2 6.5 %collective-permute-start.2 = (bf16[512,256]{1,0:T(8,128)(2,1)S(1)}, bf16[512,256]{1,0:T(8,128)(2,1)S(1)}, u32[]{:S(2)}, u32[]{:S(2)}) collective-permute-start(bf16[512,256]{1,0:T(8,128)(2,1)S(1)} %get-tuple-element.68), channel_id=1, source_target_pairs={{0,1},{1,0},{2,3},{3,2},{4,5},{5,4},{6,7},{7,6},{8,9},{9,8},{10,11... | collective-permute-start | bytes 786440 | tf_op jit(solution)/shard_map/ppermute | solution.py:326
  104.9 4.1 %fusion.9 = f32[512,2048]{1,0:T(8,128)} fusion(bf16[1024,2048]{1,0:T(8,128)(2,1)} %param.14, s32[]{:T(128)S(6)} %select_n.50, bf16[2048,256]{1,0:T(8,128)(2,1)} %attend.1, s32[]{:T(128)S(6)} %select_n.49), kind=kOutput, calls=%fused_computation.9 | convolution fusion | flops 536870912 | bytes 5505032 | tf_op jit(solution)/shard_map/dot_general | solution.py:327
  109.0 4.1 %fusion.7 = f32[512,2048]{1,0:T(8,128)} fusion(bf16[512,256]{1,0:T(8,128)(2,1)S(1)} %collective-permute-done.2, bf16[1024,2048]{1,0:T(8,128)(2,1)} %param.14, s32[]{:T(128)S(6)} %select_n.52), kind=kOutput, calls=%fused_computation.7 | convolution fusion | flops 536870912 | bytes 5505028 | tf_op jit(solution)/shard_map/dot_general | solution.py:327
  113.2 2.9 %collective-permute-start.7 = (bf16[48,2048]{1,0:T(8,128)(2,1)S(1)}, bf16[48,2048]{1,0:T(8,128)(2,1)S(1)}, u32[]{:S(2)}, u32[]{:S(2)}) collective-permute-start(bf16[48,2048]{1,0:T(8,128)(2,1)S(1)} %copy-done.26), channel_id=1, source_target_pairs={{0,12},{4,8},{8,4},{12,0},{16,28},{20,24},{24,20},{28,16},{1,13},{... | collective-permute-start | bytes 589832 | tf_op jit(solution)/shard_map/ppermute | solution.py:93
  119.3 13.1 %expert.3 = (bf16[48,2048]{1,0:T(8,128)(2,1)}, bf16[48,2048]{1,0:T(8,128)(2,1)}, bf16[48,2048]{1,0:T(8,128)(2,1)}, bf16[48,2048]{1,0:T(8,128)(2,1)}, bf16[48,204...) custom-call(bf16[48,2048]{1,0:T(8,128)(2,1)} %get-tuple-element.50.refs_0_, ...), custom_call_target="tpu_custom_call" | custom-call | flops 4831838208 | bytes 15728640 | tf_op jit(solution)/shard_map/expert/pallas_call | solution.py:139
  138.6 13.3 %expert.2 = (bf16[48,2048]{1,0:T(8,128)(2,1)}, bf16[48,2048]{1,0:T(8,128)(2,1)}, bf16[48,2048]{1,0:T(8,128)(2,1)}, bf16[48,2048]{1,0:T(8,128)(2,1)}, bf16[48,204...) custom-call(bf16[48,2048]{1,0:T(8,128)(2,1)} %get-tuple-element.34.refs_0_, ...), custom_call_target="tpu_custom_call" | custom-call | flops 4831838208 | bytes 15728640 | tf_op jit(solution)/shard_map/expert/pallas_call | solution.py:139
  151.9 3.2 %collective-permute-start.39 = (bf16[48,2048]{1,0:T(8,128)(2,1)S(1)}, bf16[48,2048]{1,0:T(8,128)(2,1)S(1)}, u32[]{:S(2)}, u32[]{:S(2)}) collective-permute-start(bf16[48,2048]{1,0:T(8,128)(2,1)S(1)} %copy-done.44), channel_id=1, source_target_pairs={{0,20},{4,16},{8,28},{12,24},{16,4},{20,0},{24,12},{28,8},{1,21},{... | collective-permute-start | bytes 589832 | tf_op jit(solution)/shard_map/ppermute | solution.py:93
  161.7 10.5 %collective-permute-done.39.refs_6_ = bf16[48,2048]{1,0:T(8,128)(2,1)S(1)} collective-permute-done((bf16[48,2048]{1,0:T(8,128)(2,1)S(1)}, bf16[48,2048]{1,0:T(8,128)(2,1)S(1)}, u32[]{:S(2)}, u32[]{:S(2)}) %collective-permute-start.39) | collective-permute-done | bytes 196640 | tf_op jit(solution)/shard_map/ppermute | solution.py:93
  172.2 3.3 %collective-permute-start.23 = (bf16[48,2048]{1,0:T(8,128)(2,1)S(1)}, bf16[48,2048]{1,0:T(8,128)(2,1)S(1)}, u32[]{:S(2)}, u32[]{:S(2)}) collective-permute-start(bf16[48,2048]{1,0:T(8,128)(2,1)S(1)} %copy-done.45), channel_id=1, source_target_pairs={{0,12},{4,8},{8,4},{12,0},{16,28},{20,24},{24,20},{28,16},{1,13},{... | collective-permute-start | bytes 589832 | tf_op jit(solution)/shard_map/ppermute | solution.py:93
  177.6 10.3 %collective-permute-done.41.refs_8_ = bf16[48,2048]{1,0:T(8,128)(2,1)S(1)} collective-permute-done((bf16[48,2048]{1,0:T(8,128)(2,1)S(1)}, bf16[48,2048]{1,0:T(8,128)(2,1)S(1)}, u32[]{:S(2)}, u32[]{:S(2)}) %collective-permute-start.41) | collective-permute-done | bytes 196640 | tf_op jit(solution)/shard_map/ppermute | solution.py:93
  189.8 5.0 %add_convert_fusion = bf16[512,2048]{1,0:T(8,128)(2,1)} fusion(f32[512,2048]{1,0:T(8,128)S(1)} %fusion.5, f32[512,2048]{1,0:T(8,128)S(1)} %copy-done, f32[512,2048]{1,0:T(8,128)} %fusion.7, bf16[512,256]{1,0:T(8,128)(2,1)S(1)} %collective-permute-done.4, bf16[1024,2048]{1,0:T(8,128)(2,1)} %param.14, s32[]{:T(128)S(6)} %select_n.56), kind=kOutput, calls=%fused_computation | convolution fusion | flops 541065216 | bytes 15990788 | tf_op jit(solution)/shard_map/dot_general | solution.py:327
  194.9 5.1 %combine.2.refs_9_ = f32[256,2048]{1,0:T(8,128)} custom-call(bf16[512,384]{1,0:T(8,128)(2,1)} %pad_maximum_fusion.2.refs_0_, bf16[48,2048]{1,0:T(8,128)(2,1)} %get-tuple-element.58.refs_1_, bf16[48,2048]{1,0:T(8,128)(2,1)} %copy-done.1, bf16[48,2048]{1,0:T(8,128)(2,1)} %copy-done.2, bf16[48,2048]{1,0:T(8,128)(2,1)} %copy-done.3, bf16[48,2048]{1,0:T(8,128)(2,1)} %copy-done.4, ...), custom_call_target="tpu_custom_call" | custom-call | flops 805306368 | bytes 4718592 | tf_op jit(solution)/shard_map/combine/pallas_call | solution.py:187
  200.0 7.2 %collective-permute-done.25.refs_6_ = bf16[48,2048]{1,0:T(8,128)(2,1)S(1)} collective-permute-done((bf16[48,2048]{1,0:T(8,128)(2,1)S(1)}, bf16[48,2048]{1,0:T(8,128)(2,1)S(1)}, u32[]{:S(2)}, u32[]{:S(2)}) %collective-permute-start.25) | collective-permute-done | bytes 196640 | tf_op jit(solution)/shard_map/ppermute | solution.py:93
  207.2 5.4 %collective-permute-done.26.refs_7_ = bf16[48,2048]{1,0:T(8,128)(2,1)S(1)} collective-permute-done((bf16[48,2048]{1,0:T(8,128)(2,1)S(1)}, bf16[48,2048]{1,0:T(8,128)(2,1)S(1)}, u32[]{:S(2)}, u32[]{:S(2)}) %collective-permute-start.26) | collective-permute-done | bytes 196640 | tf_op jit(solution)/shard_map/ppermute | solution.py:93
  212.6 4.8 %collective-permute-done.27.refs_8_ = bf16[48,2048]{1,0:T(8,128)(2,1)S(1)} collective-permute-done((bf16[48,2048]{1,0:T(8,128)(2,1)S(1)}, bf16[48,2048]{1,0:T(8,128)(2,1)S(1)}, u32[]{:S(2)}, u32[]{:S(2)}) %collective-permute-start.27) | collective-permute-done | bytes 196640 | tf_op jit(solution)/shard_map/ppermute | solution.py:93
  218.0 5.5 %combine.3 = bf16[256,2048]{1,0:T(8,128)(2,1)} custom-call(bf16[512,384]{1,0:T(8,128)(2,1)} %pad_maximum_fusion.1.refs_0_, bf16[48,2048]{1,0:T(8,128)(2,1)} %get-tuple-element.42.refs_1_, bf16[48,2048]{1,0:T(8,128)(2,1)} %copy-done.5, bf16[48,2048]{1,0:T(8,128)(2,1)} %copy-done.7, bf16[48,2048]{1,0:T(8,128)(2,1)} %copy-done.10, bf16[48,2048]{1,0:T(8,128)(2,1)} %copy-done.11, ...), custom_call_target="tpu_custom_call" | custom-call | flops 805306368 | bytes 4718592 | tf_op jit(solution)/shard_map/combine/pallas_call | solution.py:187
  (191 shorter events, 56.1 us)
Async XLA Ops:
  17.3 24.4 %collective-permute-start.32 = (bf16[48,2048]{1,0:T(8,128)(2,1)}, bf16[48,2048]{1,0:T(8,128)(2,1)S(1)}, u32[]{:S(2)}, u32[]{:S(2)}) collective-permute-start(bf16[48,2048]{1,0:T(8,128)(2,1)} %get-tuple-element.55), channel_id=1, source_target_pairs={{0,20},{4,16},{8,28},{12,24},{16,4},{20,0},{24,12},{28,8},{1,21},{... | collective-permute-start | bytes 589832 | tf_op jit(solution)/shard_map/ppermute | solution.py:93
  19.2 28.7 %collective-permute-start.33 = (bf16[48,2048]{1,0:T(8,128)(2,1)}, bf16[48,2048]{1,0:T(8,128)(2,1)S(1)}, u32[]{:S(2)}, u32[]{:S(2)}) collective-permute-start(bf16[48,2048]{1,0:T(8,128)(2,1)} %get-tuple-element.56), channel_id=1, source_target_pairs={{0,24},{4,28},{8,16},{12,20},{16,8},{20,12},{24,0},{28,4},{1,25},{... | collective-permute-start | bytes 589832 | tf_op jit(solution)/shard_map/ppermute | solution.py:93
  20.5 30.3 %collective-permute-start.34 = (bf16[48,2048]{1,0:T(8,128)(2,1)}, bf16[48,2048]{1,0:T(8,128)(2,1)S(1)}, u32[]{:S(2)}, u32[]{:S(2)}) collective-permute-start(bf16[48,2048]{1,0:T(8,128)(2,1)} %get-tuple-element.57), channel_id=1, source_target_pairs={{0,28},{4,24},{8,20},{12,16},{16,12},{20,8},{24,4},{28,0},{1,29},{... | collective-permute-start | bytes 589832 | tf_op jit(solution)/shard_map/ppermute | solution.py:93
  20.7 81.4 %collective-permute-start.15 = (bf16[2048,256]{1,0:T(8,128)(2,1)}, bf16[2048,256]{1,0:T(8,128)(2,1)}, u32[]{:S(2)}, u32[]{:S(2)}) collective-permute-start(bf16[2048,256]{1,0:T(8,128)(2,1)} %bitcast.16), channel_id=1, source_target_pairs={{0,2},{1,3},{2,0},{3,1},{4,6},{5,7},{6,4},{7,5},{8,10},{9,11},{10,... | collective-permute-start | bytes 3145736 | tf_op jit(solution)/shard_map/ppermute | solution.py:44
  25.6 77.2 %collective-permute-start.12 = (bf16[2048,256]{1,0:T(8,128)(2,1)}, bf16[2048,256]{1,0:T(8,128)(2,1)}, u32[]{:S(2)}, u32[]{:S(2)}) collective-permute-start(bf16[2048,256]{1,0:T(8,128)(2,1)} %bitcast.17), channel_id=1, source_target_pairs={{0,1},{1,0},{2,3},{3,2},{4,5},{5,4},{6,7},{7,6},{8,9},{9,8},{10,11... | collective-permute-start | bytes 3145736 | tf_op jit(solution)/shard_map/ppermute | solution.py:44
  41.7 60.6 %collective-permute-start.16 = (bf16[2048,256]{1,0:T(8,128)(2,1)}, bf16[2048,256]{1,0:T(8,128)(2,1)}, u32[]{:S(2)}, u32[]{:S(2)}) collective-permute-start(bf16[2048,256]{1,0:T(8,128)(2,1)} %bitcast.20), channel_id=1, source_target_pairs={{0,2},{1,3},{2,0},{3,1},{4,6},{5,7},{6,4},{7,5},{8,10},{9,11},{10,... | collective-permute-start | bytes 3145736 | tf_op jit(solution)/shard_map/ppermute | solution.py:44
  47.9 54.8 %collective-permute-start.17 = (bf16[256,2048]{1,0:T(8,128)(2,1)}, bf16[256,2048]{1,0:T(8,128)(2,1)}, u32[]{:S(2)}, u32[]{:S(2)}) collective-permute-start(bf16[256,2048]{1,0:T(8,128)(2,1)} %bitcast.24), channel_id=1, source_target_pairs={{0,2},{1,3},{2,0},{3,1},{4,6},{5,7},{6,4},{7,5},{8,10},{9,11},{10,... | collective-permute-start | bytes 3145736 | tf_op jit(solution)/shard_map/ppermute | solution.py:44
  70.2 23.3 %collective-permute-start.5 = (bf16[48,2048]{1,0:T(8,128)(2,1)}, bf16[48,2048]{1,0:T(8,128)(2,1)S(1)}, u32[]{:S(2)}, u32[]{:S(2)}) collective-permute-start(bf16[48,2048]{1,0:T(8,128)(2,1)} %get-tuple-element.35), channel_id=1, source_target_pairs={{0,4},{4,0},{8,12},{12,8},{16,20},{20,16},{24,28},{28,24},{1,5},{5... | collective-permute-start | bytes 589832 | tf_op jit(solution)/shard_map/ppermute | solution.py:93
  113.2 21.4 %collective-permute-start.7 = (bf16[48,2048]{1,0:T(8,128)(2,1)S(1)}, bf16[48,2048]{1,0:T(8,128)(2,1)S(1)}, u32[]{:S(2)}, u32[]{:S(2)}) collective-permute-start(bf16[48,2048]{1,0:T(8,128)(2,1)S(1)} %copy-done.26), channel_id=1, source_target_pairs={{0,12},{4,8},{8,4},{12,0},{16,28},{20,24},{24,20},{28,16},{1,13},{... | collective-permute-start | bytes 589832 | tf_op jit(solution)/shard_map/ppermute | solution.py:93
  116.0 20.2 %collective-permute-start.8 = (bf16[48,2048]{1,0:T(8,128)(2,1)S(1)}, bf16[48,2048]{1,0:T(8,128)(2,1)S(1)}, u32[]{:S(2)}, u32[]{:S(2)}) collective-permute-start(bf16[48,2048]{1,0:T(8,128)(2,1)S(1)} %copy-done.25), channel_id=1, source_target_pairs={{0,16},{4,20},{8,24},{12,28},{16,0},{20,4},{24,8},{28,12},{1,17},{... | collective-permute-start | bytes 589832 | tf_op jit(solution)/shard_map/ppermute | solution.py:93
  116.3 19.9 %collective-permute-start.9 = (bf16[48,2048]{1,0:T(8,128)(2,1)S(1)}, bf16[48,2048]{1,0:T(8,128)(2,1)S(1)}, u32[]{:S(2)}, u32[]{:S(2)}) collective-permute-start(bf16[48,2048]{1,0:T(8,128)(2,1)S(1)} %copy-done.24), channel_id=1, source_target_pairs={{0,20},{4,16},{8,28},{12,24},{16,4},{20,0},{24,12},{28,8},{1,21},{... | collective-permute-start | bytes 589832 | tf_op jit(solution)/shard_map/ppermute | solution.py:93
  118.1 20.1 %collective-permute-start.3 = (bf16[512,256]{1,0:T(8,128)(2,1)S(1)}, bf16[512,256]{1,0:T(8,128)(2,1)S(1)}, u32[]{:S(2)}, u32[]{:S(2)}) collective-permute-start(bf16[512,256]{1,0:T(8,128)(2,1)S(1)} %get-tuple-element.67), channel_id=1, source_target_pairs={{0,2},{1,3},{2,0},{3,1},{4,6},{5,7},{6,4},{7,5},{8,10},{9,11},{10,... | collective-permute-start | bytes 786440 | tf_op jit(solution)/shard_map/ppermute | solution.py:326
  134.5 20.6 %collective-permute-start.35 = (bf16[48,2048]{1,0:T(8,128)(2,1)}, bf16[48,2048]{1,0:T(8,128)(2,1)S(1)}, u32[]{:S(2)}, u32[]{:S(2)}) collective-permute-start(bf16[48,2048]{1,0:T(8,128)(2,1)} %get-tuple-element.59), channel_id=1, source_target_pairs={{0,4},{4,0},{8,12},{12,8},{16,20},{20,16},{24,28},{28,24},{1,5},{5... | collective-permute-start | bytes 589832 | tf_op jit(solution)/shard_map/ppermute | solution.py:93
  137.0 19.6 %collective-permute-start.37 = (bf16[48,2048]{1,0:T(8,128)(2,1)}, bf16[48,2048]{1,0:T(8,128)(2,1)S(1)}, u32[]{:S(2)}, u32[]{:S(2)}) collective-permute-start(bf16[48,2048]{1,0:T(8,128)(2,1)} %get-tuple-element.61), channel_id=1, source_target_pairs={{0,12},{4,8},{8,4},{12,0},{16,28},{20,24},{24,20},{28,16},{1,13},{... | collective-permute-start | bytes 589832 | tf_op jit(solution)/shard_map/ppermute | solution.py:93
  138.2 19.7 %collective-permute-start.38 = (bf16[48,2048]{1,0:T(8,128)(2,1)}, bf16[48,2048]{1,0:T(8,128)(2,1)S(1)}, u32[]{:S(2)}, u32[]{:S(2)}) collective-permute-start(bf16[48,2048]{1,0:T(8,128)(2,1)} %get-tuple-element.62), channel_id=1, source_target_pairs={{0,16},{4,20},{8,24},{12,28},{16,0},{20,4},{24,8},{28,12},{1,17},{... | collective-permute-start | bytes 589832 | tf_op jit(solution)/shard_map/ppermute | solution.py:93
  151.9 20.3 %collective-permute-start.39 = (bf16[48,2048]{1,0:T(8,128)(2,1)S(1)}, bf16[48,2048]{1,0:T(8,128)(2,1)S(1)}, u32[]{:S(2)}, u32[]{:S(2)}) collective-permute-start(bf16[48,2048]{1,0:T(8,128)(2,1)S(1)} %copy-done.44), channel_id=1, source_target_pairs={{0,20},{4,16},{8,28},{12,24},{16,4},{20,0},{24,12},{28,8},{1,21},{... | collective-permute-start | bytes 589832 | tf_op jit(solution)/shard_map/ppermute | solution.py:93
  155.1 22.5 %collective-permute-start.40 = (bf16[48,2048]{1,0:T(8,128)(2,1)S(1)}, bf16[48,2048]{1,0:T(8,128)(2,1)S(1)}, u32[]{:S(2)}, u32[]{:S(2)}) collective-permute-start(bf16[48,2048]{1,0:T(8,128)(2,1)S(1)} %copy-done.41), channel_id=1, source_target_pairs={{0,24},{4,28},{8,16},{12,20},{16,8},{20,12},{24,0},{28,4},{1,25},{... | collective-permute-start | bytes 589832 | tf_op jit(solution)/shard_map/ppermute | solution.py:93
  155.6 32.2 %collective-permute-start.41 = (bf16[48,2048]{1,0:T(8,128)(2,1)S(1)}, bf16[48,2048]{1,0:T(8,128)(2,1)S(1)}, u32[]{:S(2)}, u32[]{:S(2)}) collective-permute-start(bf16[48,2048]{1,0:T(8,128)(2,1)S(1)} %copy-done.38), channel_id=1, source_target_pairs={{0,28},{4,24},{8,20},{12,16},{16,12},{20,8},{24,4},{28,0},{1,29},{... | collective-permute-start | bytes 589832 | tf_op jit(solution)/shard_map/ppermute | solution.py:93
  156.5 31.4 %collective-permute-start.21 = (bf16[48,2048]{1,0:T(8,128)(2,1)}, bf16[48,2048]{1,0:T(8,128)(2,1)S(1)}, u32[]{:S(2)}, u32[]{:S(2)}) collective-permute-start(bf16[48,2048]{1,0:T(8,128)(2,1)} %get-tuple-element.43), channel_id=1, source_target_pairs={{0,4},{4,0},{8,12},{12,8},{16,20},{20,16},{24,28},{28,24},{1,5},{5... | collective-permute-start | bytes 589832 | tf_op jit(solution)/shard_map/ppermute | solution.py:93
  157.9 30.8 %collective-permute-start.22 = (bf16[48,2048]{1,0:T(8,128)(2,1)}, bf16[48,2048]{1,0:T(8,128)(2,1)S(1)}, u32[]{:S(2)}, u32[]{:S(2)}) collective-permute-start(bf16[48,2048]{1,0:T(8,128)(2,1)} %get-tuple-element.44), channel_id=1, source_target_pairs={{0,8},{4,12},{8,0},{12,4},{16,24},{20,28},{24,16},{28,20},{1,9},{5... | collective-permute-start | bytes 589832 | tf_op jit(solution)/shard_map/ppermute | solution.py:93
  172.2 27.7 %collective-permute-start.23 = (bf16[48,2048]{1,0:T(8,128)(2,1)S(1)}, bf16[48,2048]{1,0:T(8,128)(2,1)S(1)}, u32[]{:S(2)}, u32[]{:S(2)}) collective-permute-start(bf16[48,2048]{1,0:T(8,128)(2,1)S(1)} %copy-done.45), channel_id=1, source_target_pairs={{0,12},{4,8},{8,4},{12,0},{16,28},{20,24},{24,20},{28,16},{1,13},{... | collective-permute-start | bytes 589832 | tf_op jit(solution)/shard_map/ppermute | solution.py:93
  177.6 22.4 %collective-permute-start.24 = (bf16[48,2048]{1,0:T(8,128)(2,1)S(1)}, bf16[48,2048]{1,0:T(8,128)(2,1)S(1)}, u32[]{:S(2)}, u32[]{:S(2)}) collective-permute-start(bf16[48,2048]{1,0:T(8,128)(2,1)S(1)} %copy-done.43), channel_id=1, source_target_pairs={{0,16},{4,20},{8,24},{12,28},{16,0},{20,4},{24,8},{28,12},{1,17},{... | collective-permute-start | bytes 589832 | tf_op jit(solution)/shard_map/ppermute | solution.py:93
  187.9 24.7 %collective-permute-start.26 = (bf16[48,2048]{1,0:T(8,128)(2,1)S(1)}, bf16[48,2048]{1,0:T(8,128)(2,1)S(1)}, u32[]{:S(2)}, u32[]{:S(2)}) collective-permute-start(bf16[48,2048]{1,0:T(8,128)(2,1)S(1)} %copy-done.40), channel_id=1, source_target_pairs={{0,24},{4,28},{8,16},{12,20},{16,8},{20,12},{24,0},{28,4},{1,25},{... | collective-permute-start | bytes 589832 | tf_op jit(solution)/shard_map/ppermute | solution.py:93
  188.7 28.6 %collective-permute-start.27 = (bf16[48,2048]{1,0:T(8,128)(2,1)S(1)}, bf16[48,2048]{1,0:T(8,128)(2,1)S(1)}, u32[]{:S(2)}, u32[]{:S(2)}) collective-permute-start(bf16[48,2048]{1,0:T(8,128)(2,1)S(1)} %copy-done.39), channel_id=1, source_target_pairs={{0,28},{4,24},{8,20},{12,16},{16,12},{20,8},{24,4},{28,0},{1,29},{... | collective-permute-start | bytes 589832 | tf_op jit(solution)/shard_map/ppermute | solution.py:93
  (68 other events, 1194.9 us)

commit v2 on v1

--- a/solution.py
+++ b/solution.py
@@ -99,7 +99,14 @@
 def expert_kernel(*refs, peers, count):
     row_refs, sources, out_refs = refs[:peers], refs[peers : peers + count], refs[peers + count :]
     out_refs, held = out_refs[:peers], out_refs[peers:]
-    rows_held, total_ref, arrivals = held[count:]
+    rows_held, hidden_ref, down_ref, arrivals = held[-4:]
+    units = sources[2].shape[0]
+    down_places = [down_ref.at[pl.ds(units * part, units)] for part in range(count // 3)]
+    held = [
+        place
+        for part, down_place in enumerate(down_places)
+        for place in (held[2 * part], held[2 * part + 1], down_place)
+    ]
     row_copies = [
         pltpu.make_async_copy(source, rows_held.at[peer], arrivals.at[count + peer])
         for peer, source in enumerate(row_refs)
@@ -108,26 +115,35 @@
         pltpu.make_async_copy(source, place, arrivals.at[number])
         for number, (source, place) in enumerate(zip(sources, held))
     ]
-    for copy in row_copies + copies:
+    ahead = [copies[part + half] for part in range(0, count, 3) for half in range(2)]
+    ahead = ahead + [copies[part + 2] for part in range(0, count, 3)]
+    for copy in row_copies + ahead[:2]:
         copy.start()
     for copy in row_copies:
         copy.wait()
+    for copy in ahead[2:4]:
+        copy.start()
+    ahead = ahead[4:]
     chunk, width = row_refs[0].shape
     rows = rows_held[...].reshape(peers * chunk, width)
     for number in range(0, count, 3):
         copies[number].wait()
         gate_value = jnp.dot(rows, held[number][...], preferred_element_type=jnp.float32)
         copies[number + 1].wait()
+        fresh, ahead = (ahead[:3], ahead[3:]) if number + 3 < count else (ahead, [])
+        for copy in fresh:
+            copy.start()
         up_value = jnp.dot(rows, held[number + 1][...], preferred_element_type=jnp.float32)
         hidden = (gate_value / (1.0 + jnp.exp(-gate_value)) * up_value).astype(jnp.bfloat16)
-        copies[number + 2].wait()
-        part = jnp.dot(hidden, held[number + 2][...], preferred_element_type=jnp.float32)
-        if number + 3 < count:
-            total_ref[...] = part if number == 0 else total_ref[...] + part
-        else:
-            total = (total_ref[...] + part if number else part).astype(jnp.bfloat16)
-            for peer in range(peers):
-                out_refs[peer][...] = total[peer * chunk : (peer + 1) * chunk]
+        first = number // 3 * units
+        hidden_ref[:, first : first + units] = hidden
+    for number in range(2, count, 3):
+        copies[number].wait()
+    total = jnp.dot(
+        hidden_ref[...], down_ref[...], preferred_element_type=jnp.float32
+    ).astype(jnp.bfloat16)
+    for peer in range(peers):
+        out_refs[peer][...] = total[peer * chunk : (peer + 1) * chunk]
 
 
 def expert_chunk(blocks, parts):
@@ -140,10 +156,13 @@
         lambda *refs: expert_kernel(*refs, peers=peers, count=len(flat)),
         out_shape=[jax.ShapeDtypeStruct((chunk, width), jnp.bfloat16)] * peers,
         in_specs=[pl.BlockSpec(memory_space=pl.ANY)] * (peers + len(flat)),
-        scratch_shapes=[pltpu.VMEM(array.shape, array.dtype) for array in flat]
+        scratch_shapes=[
+            pltpu.VMEM(array.shape, array.dtype) for part in parts for array in part[:2]
+        ]
         + [
             pltpu.VMEM((peers, chunk, width), jnp.bfloat16),
-            pltpu.VMEM((row_count, width), jnp.float32),
+            pltpu.VMEM((row_count, hidden_units), jnp.bfloat16),
+            pltpu.VMEM((hidden_units, width), jnp.bfloat16),
             pltpu.SemaphoreType.DMA((len(flat) + peers,)),
         ],
         cost_estimate=pl.CostEstimate(
@@ -157,24 +176,15 @@
 
 def combine_kernel(shares_ref, *refs, peers):
     block_refs, rest = refs[:peers], refs[peers:]
-    out_ref, held, arrivals = rest[-3:]
-    copies = [
-        pltpu.make_async_copy(source, held.at[peer], arrivals.at[peer])
-        for peer, source in enumerate(block_refs)
-    ]
-    for copy in copies:
-        copy.start()
-    for copy in copies:
-        copy.wait()
-    chunk, width = block_refs[0].shape
+    out_ref = rest[-1]
     both = jnp.dot(
         shares_ref[...],
-        held[...].reshape(peers * chunk, width),
+        jnp.concatenate([block[...] for block in block_refs], 0),
         preferred_element_type=jnp.float32,
     )
     row_count = out_ref.shape[0]
     total = both[:row_count] + both[row_count:]
-    if len(rest) > 3:
+    if len(rest) > 1:
         total = total + rest[0][...]
     out_ref[...] = total.astype(out_ref.dtype)
 
@@ -183,15 +193,15 @@
     peers = len(blocks)
     chunk, width = blocks[0].shape
     row_count = shares.shape[0] // 2
-    whole = pl.BlockSpec(memory_space=pltpu.VMEM)
+    columns = width // 4
     return pl.pallas_call(
         lambda *refs: combine_kernel(*refs, peers=peers),
         out_shape=jax.ShapeDtypeStruct((row_count, width), kind),
-        in_specs=[whole] + [pl.BlockSpec(memory_space=pl.ANY)] * peers + [whole] * len(earlier),
-        scratch_shapes=[
-            pltpu.VMEM((peers, chunk, width), jnp.bfloat16),
-            pltpu.SemaphoreType.DMA((peers,)),
-        ],
+        grid=(width // columns,),
+        in_specs=[pl.BlockSpec(shares.shape, lambda i: (0, 0))]
+        + [pl.BlockSpec((chunk, columns), lambda i: (0, i))] * peers
+        + [pl.BlockSpec((row_count, columns), lambda i: (0, i))] * len(earlier),
+        out_specs=pl.BlockSpec((row_count, columns), lambda i: (0, i)),
         cost_estimate=pl.CostEstimate(
             flops=4 * row_count * peers * chunk * width,
             bytes_accessed=2 * peers * chunk * width + 6 * row_count * width,

time: 224 us -> 223 us (level)
  no operation moved by 1% of the time
where the time goes in v2:
time: 223 us; the launch traced here: 222 us
  starting transfers between devices  76.1 us (34%)
  Pallas kernels  59.7 us (27%)
  waiting for transfers between devices  56.9 us (26%)
  matrix products  15.8 us (7%)
  other arithmetic  6.35 us (3%)
  local copies, waits for them, and re-layouts  6.1 us (3%)
    ppermute x28, waiting for transfers between devices, exchange(): lax.ppermute(blocks[k], axis, [(i, i ^ k) for i in range(count)])  56.4 us
    ppermute x28, starting transfers between devices, exchange(): lax.ppermute(blocks[k], axis, [(i, i ^ k) for i in range(count)])  39.1 us
    pallas_call x2, Pallas kernels, expert_chunk(): pl.pallas_call(lambda *refs: expert_kernel(*refs, peers=peers, count=len(...  25.4 us
    ppermute x9, starting transfers between devices, gathered_parts(): lax.ppermute(block, axis, pairs)  21.1 us
    pallas_call x1, Pallas kernels, attend(): pl.pallas_call(lambda *refs: attend_kernel(*refs, group_size=group_size),...  20.4 us
    dot_general x4, matrix products, layer(): jnp.dot(rows, lax.dynamic_slice_in_dim(out_weight, (mine ^ other) * width...  15 us
    pallas_call x2, Pallas kernels, combine(): pl.pallas_call(lambda *refs: combine_kernel(*refs, peers=peers), out_shap...  9.92 us
    ppermute x3, starting transfers between devices, layer(): rows = lax.ppermute(rows, 'tp', [(i, i ^ other) for i in range(tp_count)])  9.81 us
  transfers between devices with their start and end apart: 42, of which 12 were waited for; matrix products, arithmetic and copies ran while one was open for 10% of the time, Pallas kernels for 23%

profile of v2, /device:TPU:9, one launch (start us, length us, event | category | flops | bytes accessed | tf_op | source)
XLA Modules:
  0.0 222.1 jit_solution(11174121991874972375)
XLA Ops:
  2.2 4.0 %dispatch.1 = (bf16[48,2048]{1,0:T(8,128)(2,1)}, bf16[48,2048]{1,0:T(8,128)(2,1)}, bf16[48,2048]{1,0:T(8,128)(2,1)}, bf16[48,2048]{1,0:T(8,128)(2,1)}, bf16[48,2...) custom-call(bf16[256,2048]{1,0:T(8,128)(2,1)} %tokens_ref.1, ...), custom_call_target="tpu_custom_call" | custom-call | flops 805306368 | bytes 4194304 | tf_op jit(solution)/shard_map/dispatch/pallas_call | solution.py:77
  10.3 4.2 %collective-permute-start.1 = (bf16[128,128]{1,0:T(8,128)(2,1)S(1)}, bf16[128,128]{1,0:T(8,128)(2,1)S(1)}, u32[]{:S(2)}, u32[]{:S(2)}) collective-permute-start(bf16[128,128]{1,0:T(8,128)(2,1)S(1)} %get-tuple-element.76), channel_id=1, source_target_pairs={{4,0},{8,4},{12,8},{16,12},{20,16},{24,20},{28,24},{5,1},{9,5},{13... | collective-permute-start | bytes 98312 | tf_op jit(solution)/shard_map/ppermute | solution.py:30
  21.9 3.6 %collective-permute-done.31.refs_4_ = bf16[48,2048]{1,0:T(8,128)(2,1)S(1)} collective-permute-done((bf16[48,2048]{1,0:T(8,128)(2,1)}, bf16[48,2048]{1,0:T(8,128)(2,1)S(1)}, u32[]{:S(2)}, u32[]{:S(2)}) %collective-permute-start.31) | collective-permute-done | bytes 196640 | tf_op jit(solution)/shard_map/ppermute | solution.py:93
  25.6 16.1 %collective-permute-start.12 = (bf16[2048,256]{1,0:T(8,128)(2,1)}, bf16[2048,256]{1,0:T(8,128)(2,1)}, u32[]{:S(2)}, u32[]{:S(2)}) collective-permute-start(bf16[2048,256]{1,0:T(8,128)(2,1)} %bitcast.17), channel_id=1, source_target_pairs={{0,1},{1,0},{2,3},{3,2},{4,5},{5,4},{6,7},{7,6},{8,9},{9,8},{10,11... | collective-permute-start | bytes 3145736 | tf_op jit(solution)/shard_map/ppermute | solution.py:44
  42.9 5.0 %collective-permute-done.33.refs_6_ = bf16[48,2048]{1,0:T(8,128)(2,1)S(1)} collective-permute-done((bf16[48,2048]{1,0:T(8,128)(2,1)}, bf16[48,2048]{1,0:T(8,128)(2,1)S(1)}, u32[]{:S(2)}, u32[]{:S(2)}) %collective-permute-start.33) | collective-permute-done | bytes 196640 | tf_op jit(solution)/shard_map/ppermute | solution.py:93
  51.4 5.8 %collective-permute-start.10 = (bf16[48,2048]{1,0:T(8,128)(2,1)}, bf16[48,2048]{1,0:T(8,128)(2,1)S(1)}, u32[]{:S(2)}, u32[]{:S(2)}) collective-permute-start(bf16[48,2048]{1,0:T(8,128)(2,1)} %get-tuple-element.40), channel_id=1, source_target_pairs={{0,24},{4,28},{8,16},{12,20},{16,8},{20,12},{24,0},{28,4},{1,25},{... | collective-permute-start | bytes 589832 | tf_op jit(solution)/shard_map/ppermute | solution.py:93
  59.1 3.3 %collective-permute-done.10.refs_6_ = bf16[48,2048]{1,0:T(8,128)(2,1)S(1)} collective-permute-done((bf16[48,2048]{1,0:T(8,128)(2,1)}, bf16[48,2048]{1,0:T(8,128)(2,1)S(1)}, u32[]{:S(2)}, u32[]{:S(2)}) %collective-permute-start.10) | collective-permute-done | bytes 196640 | tf_op jit(solution)/shard_map/ppermute | solution.py:93
  71.9 20.4 %attend.1 = bf16[2048,256]{1,0:T(8,128)(2,1)} custom-call(s32[2]{0:T(128)} %pad_add_fusion.refs_0_, f32[4]{0:T(128)} %dynamic-slice_multiply_fusion.refs_1_, bf16[2048,256]{1,0:T(8,128)(2,1)} %refs_2_.1, bf16[2304,128]{1,0:T(8,128)(2,1)} %pad_maximum_fusion.refs_3_), custom_call_target="tpu_custom_call" | custom-call | flops 1610612736 | bytes 2686976 | tf_op jit(solution)/shard_map/attend/pallas_call | solution.py:272
  94.2 6.5 %collective-permute-start.2 = (bf16[512,256]{1,0:T(8,128)(2,1)S(1)}, bf16[512,256]{1,0:T(8,128)(2,1)S(1)}, u32[]{:S(2)}, u32[]{:S(2)}) collective-permute-start(bf16[512,256]{1,0:T(8,128)(2,1)S(1)} %get-tuple-element.68), channel_id=1, source_target_pairs={{0,1},{1,0},{2,3},{3,2},{4,5},{5,4},{6,7},{7,6},{8,9},{9,8},{10,11... | collective-permute-start | bytes 786440 | tf_op jit(solution)/shard_map/ppermute | solution.py:336
  104.9 4.1 %fusion.9 = f32[512,2048]{1,0:T(8,128)} fusion(bf16[1024,2048]{1,0:T(8,128)(2,1)} %param.14, s32[]{:T(128)S(6)} %select_n.50, bf16[2048,256]{1,0:T(8,128)(2,1)} %attend.1, s32[]{:T(128)S(6)} %select_n.49), kind=kOutput, calls=%fused_computation.9 | convolution fusion | flops 536870912 | bytes 5505032 | tf_op jit(solution)/shard_map/dot_general | solution.py:337
  109.0 4.1 %fusion.7 = f32[512,2048]{1,0:T(8,128)} fusion(bf16[512,256]{1,0:T(8,128)(2,1)S(1)} %collective-permute-done.2, bf16[1024,2048]{1,0:T(8,128)(2,1)} %param.14, s32[]{:T(128)S(6)} %select_n.52), kind=kOutput, calls=%fused_computation.7 | convolution fusion | flops 536870912 | bytes 5505028 | tf_op jit(solution)/shard_map/dot_general | solution.py:337
  113.2 2.9 %collective-permute-start.7 = (bf16[48,2048]{1,0:T(8,128)(2,1)S(1)}, bf16[48,2048]{1,0:T(8,128)(2,1)S(1)}, u32[]{:S(2)}, u32[]{:S(2)}) collective-permute-start(bf16[48,2048]{1,0:T(8,128)(2,1)S(1)} %copy-done.26), channel_id=1, source_target_pairs={{0,12},{4,8},{8,4},{12,0},{16,28},{20,24},{24,20},{28,16},{1,13},{... | collective-permute-start | bytes 589832 | tf_op jit(solution)/shard_map/ppermute | solution.py:93
  119.3 12.6 %expert.3 = (bf16[48,2048]{1,0:T(8,128)(2,1)}, bf16[48,2048]{1,0:T(8,128)(2,1)}, bf16[48,2048]{1,0:T(8,128)(2,1)}, bf16[48,2048]{1,0:T(8,128)(2,1)}, bf16[48,204...) custom-call(bf16[48,2048]{1,0:T(8,128)(2,1)} %get-tuple-element.50.refs_0_, ...), custom_call_target="tpu_custom_call" | custom-call | flops 4831838208 | bytes 15728640 | tf_op jit(solution)/shard_map/expert/pallas_call | solution.py:155
  138.1 12.8 %expert.2 = (bf16[48,2048]{1,0:T(8,128)(2,1)}, bf16[48,2048]{1,0:T(8,128)(2,1)}, bf16[48,2048]{1,0:T(8,128)(2,1)}, bf16[48,2048]{1,0:T(8,128)(2,1)}, bf16[48,204...) custom-call(bf16[48,2048]{1,0:T(8,128)(2,1)} %get-tuple-element.34.refs_0_, ...), custom_call_target="tpu_custom_call" | custom-call | flops 4831838208 | bytes 15728640 | tf_op jit(solution)/shard_map/expert/pallas_call | solution.py:155
  151.0 3.2 %collective-permute-start.39 = (bf16[48,2048]{1,0:T(8,128)(2,1)S(1)}, bf16[48,2048]{1,0:T(8,128)(2,1)S(1)}, u32[]{:S(2)}, u32[]{:S(2)}) collective-permute-start(bf16[48,2048]{1,0:T(8,128)(2,1)S(1)} %copy-done.44), channel_id=1, source_target_pairs={{0,20},{4,16},{8,28},{12,24},{16,4},{20,0},{24,12},{28,8},{1,21},{... | collective-permute-start | bytes 589832 | tf_op jit(solution)/shard_map/ppermute | solution.py:93
  160.8 10.5 %collective-permute-done.39.refs_6_ = bf16[48,2048]{1,0:T(8,128)(2,1)S(1)} collective-permute-done((bf16[48,2048]{1,0:T(8,128)(2,1)S(1)}, bf16[48,2048]{1,0:T(8,128)(2,1)S(1)}, u32[]{:S(2)}, u32[]{:S(2)}) %collective-permute-start.39) | collective-permute-done | bytes 196640 | tf_op jit(solution)/shard_map/ppermute | solution.py:93
  171.3 3.3 %collective-permute-start.23 = (bf16[48,2048]{1,0:T(8,128)(2,1)S(1)}, bf16[48,2048]{1,0:T(8,128)(2,1)S(1)}, u32[]{:S(2)}, u32[]{:S(2)}) collective-permute-start(bf16[48,2048]{1,0:T(8,128)(2,1)S(1)} %copy-done.45), channel_id=1, source_target_pairs={{0,12},{4,8},{8,4},{12,0},{16,28},{20,24},{24,20},{28,16},{1,13},{... | collective-permute-start | bytes 589832 | tf_op jit(solution)/shard_map/ppermute | solution.py:93
  176.6 10.3 %collective-permute-done.41.refs_8_ = bf16[48,2048]{1,0:T(8,128)(2,1)S(1)} collective-permute-done((bf16[48,2048]{1,0:T(8,128)(2,1)S(1)}, bf16[48,2048]{1,0:T(8,128)(2,1)S(1)}, u32[]{:S(2)}, u32[]{:S(2)}) %collective-permute-start.41) | collective-permute-done | bytes 196640 | tf_op jit(solution)/shard_map/ppermute | solution.py:93
  188.9 5.0 %add_convert_fusion = bf16[512,2048]{1,0:T(8,128)(2,1)} fusion(f32[512,2048]{1,0:T(8,128)S(1)} %fusion.5, f32[512,2048]{1,0:T(8,128)S(1)} %copy-done, f32[512,2048]{1,0:T(8,128)} %fusion.7, bf16[512,256]{1,0:T(8,128)(2,1)S(1)} %collective-permute-done.4, bf16[1024,2048]{1,0:T(8,128)(2,1)} %param.14, s32[]{:T(128)S(6)} %select_n.56), kind=kOutput, calls=%fused_computation | convolution fusion | flops 541065216 | bytes 15990788 | tf_op jit(solution)/shard_map/dot_general | solution.py:337
  193.9 4.9 %combine.2.refs_9_ = f32[256,2048]{1,0:T(8,128)} custom-call(bf16[512,384]{1,0:T(8,128)(2,1)} %pad_maximum_fusion.2.refs_0_, bf16[48,2048]{1,0:T(8,128)(2,1)} %get-tuple-element.58.refs_1_, bf16[48,2048]{1,0:T(8,128)(2,1)} %copy-done.1, bf16[48,2048]{1,0:T(8,128)(2,1)} %copy-done.2, bf16[48,2048]{1,0:T(8,128)(2,1)} %copy-done.3, bf16[48,2048]{1,0:T(8,128)(2,1)} %copy-done.4, ...), custom_call_target="tpu_custom_call" | custom-call | flops 805306368 | bytes 4718592 | tf_op jit(solution)/shard_map/combine/pallas_call | solution.py:197
  198.8 7.4 %collective-permute-done.25.refs_6_ = bf16[48,2048]{1,0:T(8,128)(2,1)S(1)} collective-permute-done((bf16[48,2048]{1,0:T(8,128)(2,1)S(1)}, bf16[48,2048]{1,0:T(8,128)(2,1)S(1)}, u32[]{:S(2)}, u32[]{:S(2)}) %collective-permute-start.25) | collective-permute-done | bytes 196640 | tf_op jit(solution)/shard_map/ppermute | solution.py:93
  206.2 5.4 %collective-permute-done.26.refs_7_ = bf16[48,2048]{1,0:T(8,128)(2,1)S(1)} collective-permute-done((bf16[48,2048]{1,0:T(8,128)(2,1)S(1)}, bf16[48,2048]{1,0:T(8,128)(2,1)S(1)}, u32[]{:S(2)}, u32[]{:S(2)}) %collective-permute-start.26) | collective-permute-done | bytes 196640 | tf_op jit(solution)/shard_map/ppermute | solution.py:93
  211.6 4.8 %collective-permute-done.27.refs_8_ = bf16[48,2048]{1,0:T(8,128)(2,1)S(1)} collective-permute-done((bf16[48,2048]{1,0:T(8,128)(2,1)S(1)}, bf16[48,2048]{1,0:T(8,128)(2,1)S(1)}, u32[]{:S(2)}, u32[]{:S(2)}) %collective-permute-start.27) | collective-permute-done | bytes 196640 | tf_op jit(solution)/shard_map/ppermute | solution.py:93
  217.1 5.0 %combine.3 = bf16[256,2048]{1,0:T(8,128)(2,1)} custom-call(bf16[512,384]{1,0:T(8,128)(2,1)} %pad_maximum_fusion.1.refs_0_, bf16[48,2048]{1,0:T(8,128)(2,1)} %get-tuple-element.42.refs_1_, bf16[48,2048]{1,0:T(8,128)(2,1)} %copy-done.5, bf16[48,2048]{1,0:T(8,128)(2,1)} %copy-done.7, bf16[48,2048]{1,0:T(8,128)(2,1)} %copy-done.10, bf16[48,2048]{1,0:T(8,128)(2,1)} %copy-done.11, ...), custom_call_target="tpu_custom_call" | custom-call | flops 805306368 | bytes 4718592 | tf_op jit(solution)/shard_map/combine/pallas_call | solution.py:197
  (191 shorter events, 56.1 us)
Async XLA Ops:
  17.3 24.4 %collective-permute-start.32 = (bf16[48,2048]{1,0:T(8,128)(2,1)}, bf16[48,2048]{1,0:T(8,128)(2,1)S(1)}, u32[]{:S(2)}, u32[]{:S(2)}) collective-permute-start(bf16[48,2048]{1,0:T(8,128)(2,1)} %get-tuple-element.55), channel_id=1, source_target_pairs={{0,20},{4,16},{8,28},{12,24},{16,4},{20,0},{24,12},{28,8},{1,21},{... | collective-permute-start | bytes 589832 | tf_op jit(solution)/shard_map/ppermute | solution.py:93
  19.2 28.7 %collective-permute-start.33 = (bf16[48,2048]{1,0:T(8,128)(2,1)}, bf16[48,2048]{1,0:T(8,128)(2,1)S(1)}, u32[]{:S(2)}, u32[]{:S(2)}) collective-permute-start(bf16[48,2048]{1,0:T(8,128)(2,1)} %get-tuple-element.56), channel_id=1, source_target_pairs={{0,24},{4,28},{8,16},{12,20},{16,8},{20,12},{24,0},{28,4},{1,25},{... | collective-permute-start | bytes 589832 | tf_op jit(solution)/shard_map/ppermute | solution.py:93
  20.5 30.3 %collective-permute-start.34 = (bf16[48,2048]{1,0:T(8,128)(2,1)}, bf16[48,2048]{1,0:T(8,128)(2,1)S(1)}, u32[]{:S(2)}, u32[]{:S(2)}) collective-permute-start(bf16[48,2048]{1,0:T(8,128)(2,1)} %get-tuple-element.57), channel_id=1, source_target_pairs={{0,28},{4,24},{8,20},{12,16},{16,12},{20,8},{24,4},{28,0},{1,29},{... | collective-permute-start | bytes 589832 | tf_op jit(solution)/shard_map/ppermute | solution.py:93
  20.7 81.4 %collective-permute-start.15 = (bf16[2048,256]{1,0:T(8,128)(2,1)}, bf16[2048,256]{1,0:T(8,128)(2,1)}, u32[]{:S(2)}, u32[]{:S(2)}) collective-permute-start(bf16[2048,256]{1,0:T(8,128)(2,1)} %bitcast.16), channel_id=1, source_target_pairs={{0,2},{1,3},{2,0},{3,1},{4,6},{5,7},{6,4},{7,5},{8,10},{9,11},{10,... | collective-permute-start | bytes 3145736 | tf_op jit(solution)/shard_map/ppermute | solution.py:44
  25.6 77.2 %collective-permute-start.12 = (bf16[2048,256]{1,0:T(8,128)(2,1)}, bf16[2048,256]{1,0:T(8,128)(2,1)}, u32[]{:S(2)}, u32[]{:S(2)}) collective-permute-start(bf16[2048,256]{1,0:T(8,128)(2,1)} %bitcast.17), channel_id=1, source_target_pairs={{0,1},{1,0},{2,3},{3,2},{4,5},{5,4},{6,7},{7,6},{8,9},{9,8},{10,11... | collective-permute-start | bytes 3145736 | tf_op jit(solution)/shard_map/ppermute | solution.py:44
  41.7 60.6 %collective-permute-start.16 = (bf16[2048,256]{1,0:T(8,128)(2,1)}, bf16[2048,256]{1,0:T(8,128)(2,1)}, u32[]{:S(2)}, u32[]{:S(2)}) collective-permute-start(bf16[2048,256]{1,0:T(8,128)(2,1)} %bitcast.20), channel_id=1, source_target_pairs={{0,2},{1,3},{2,0},{3,1},{4,6},{5,7},{6,4},{7,5},{8,10},{9,11},{10,... | collective-permute-start | bytes 3145736 | tf_op jit(solution)/shard_map/ppermute | solution.py:44
  47.9 54.8 %collective-permute-start.17 = (bf16[256,2048]{1,0:T(8,128)(2,1)}, bf16[256,2048]{1,0:T(8,128)(2,1)}, u32[]{:S(2)}, u32[]{:S(2)}) collective-permute-start(bf16[256,2048]{1,0:T(8,128)(2,1)} %bitcast.24), channel_id=1, source_target_pairs={{0,2},{1,3},{2,0},{3,1},{4,6},{5,7},{6,4},{7,5},{8,10},{9,11},{10,... | collective-permute-start | bytes 3145736 | tf_op jit(solution)/shard_map/ppermute | solution.py:44
  70.2 23.3 %collective-permute-start.5 = (bf16[48,2048]{1,0:T(8,128)(2,1)}, bf16[48,2048]{1,0:T(8,128)(2,1)S(1)}, u32[]{:S(2)}, u32[]{:S(2)}) collective-permute-start(bf16[48,2048]{1,0:T(8,128)(2,1)} %get-tuple-element.35), channel_id=1, source_target_pairs={{0,4},{4,0},{8,12},{12,8},{16,20},{20,16},{24,28},{28,24},{1,5},{5... | collective-permute-start | bytes 589832 | tf_op jit(solution)/shard_map/ppermute | solution.py:93
  113.2 20.9 %collective-permute-start.7 = (bf16[48,2048]{1,0:T(8,128)(2,1)S(1)}, bf16[48,2048]{1,0:T(8,128)(2,1)S(1)}, u32[]{:S(2)}, u32[]{:S(2)}) collective-permute-start(bf16[48,2048]{1,0:T(8,128)(2,1)S(1)} %copy-done.26), channel_id=1, source_target_pairs={{0,12},{4,8},{8,4},{12,0},{16,28},{20,24},{24,20},{28,16},{1,13},{... | collective-permute-start | bytes 589832 | tf_op jit(solution)/shard_map/ppermute | solution.py:93
  116.0 19.7 %collective-permute-start.8 = (bf16[48,2048]{1,0:T(8,128)(2,1)S(1)}, bf16[48,2048]{1,0:T(8,128)(2,1)S(1)}, u32[]{:S(2)}, u32[]{:S(2)}) collective-permute-start(bf16[48,2048]{1,0:T(8,128)(2,1)S(1)} %copy-done.25), channel_id=1, source_target_pairs={{0,16},{4,20},{8,24},{12,28},{16,0},{20,4},{24,8},{28,12},{1,17},{... | collective-permute-start | bytes 589832 | tf_op jit(solution)/shard_map/ppermute | solution.py:93
  116.3 19.4 %collective-permute-start.9 = (bf16[48,2048]{1,0:T(8,128)(2,1)S(1)}, bf16[48,2048]{1,0:T(8,128)(2,1)S(1)}, u32[]{:S(2)}, u32[]{:S(2)}) collective-permute-start(bf16[48,2048]{1,0:T(8,128)(2,1)S(1)} %copy-done.24), channel_id=1, source_target_pairs={{0,20},{4,16},{8,28},{12,24},{16,4},{20,0},{24,12},{28,8},{1,21},{... | collective-permute-start | bytes 589832 | tf_op jit(solution)/shard_map/ppermute | solution.py:93
  118.1 19.6 %collective-permute-start.3 = (bf16[512,256]{1,0:T(8,128)(2,1)S(1)}, bf16[512,256]{1,0:T(8,128)(2,1)S(1)}, u32[]{:S(2)}, u32[]{:S(2)}) collective-permute-start(bf16[512,256]{1,0:T(8,128)(2,1)S(1)} %get-tuple-element.67), channel_id=1, source_target_pairs={{0,2},{1,3},{2,0},{3,1},{4,6},{5,7},{6,4},{7,5},{8,10},{9,11},{10,... | collective-permute-start | bytes 786440 | tf_op jit(solution)/shard_map/ppermute | solution.py:336
  134.1 20.1 %collective-permute-start.35 = (bf16[48,2048]{1,0:T(8,128)(2,1)}, bf16[48,2048]{1,0:T(8,128)(2,1)S(1)}, u32[]{:S(2)}, u32[]{:S(2)}) collective-permute-start(bf16[48,2048]{1,0:T(8,128)(2,1)} %get-tuple-element.59), channel_id=1, source_target_pairs={{0,4},{4,0},{8,12},{12,8},{16,20},{20,16},{24,28},{28,24},{1,5},{5... | collective-permute-start | bytes 589832 | tf_op jit(solution)/shard_map/ppermute | solution.py:93
  137.7 19.2 %collective-permute-start.38 = (bf16[48,2048]{1,0:T(8,128)(2,1)}, bf16[48,2048]{1,0:T(8,128)(2,1)S(1)}, u32[]{:S(2)}, u32[]{:S(2)}) collective-permute-start(bf16[48,2048]{1,0:T(8,128)(2,1)} %get-tuple-element.62), channel_id=1, source_target_pairs={{0,16},{4,20},{8,24},{12,28},{16,0},{20,4},{24,8},{28,12},{1,17},{... | collective-permute-start | bytes 589832 | tf_op jit(solution)/shard_map/ppermute | solution.py:93
  151.0 20.3 %collective-permute-start.39 = (bf16[48,2048]{1,0:T(8,128)(2,1)S(1)}, bf16[48,2048]{1,0:T(8,128)(2,1)S(1)}, u32[]{:S(2)}, u32[]{:S(2)}) collective-permute-start(bf16[48,2048]{1,0:T(8,128)(2,1)S(1)} %copy-done.44), channel_id=1, source_target_pairs={{0,20},{4,16},{8,28},{12,24},{16,4},{20,0},{24,12},{28,8},{1,21},{... | collective-permute-start | bytes 589832 | tf_op jit(solution)/shard_map/ppermute | solution.py:93
  154.2 22.5 %collective-permute-start.40 = (bf16[48,2048]{1,0:T(8,128)(2,1)S(1)}, bf16[48,2048]{1,0:T(8,128)(2,1)S(1)}, u32[]{:S(2)}, u32[]{:S(2)}) collective-permute-start(bf16[48,2048]{1,0:T(8,128)(2,1)S(1)} %copy-done.41), channel_id=1, source_target_pairs={{0,24},{4,28},{8,16},{12,20},{16,8},{20,12},{24,0},{28,4},{1,25},{... | collective-permute-start | bytes 589832 | tf_op jit(solution)/shard_map/ppermute | solution.py:93
  154.7 32.2 %collective-permute-start.41 = (bf16[48,2048]{1,0:T(8,128)(2,1)S(1)}, bf16[48,2048]{1,0:T(8,128)(2,1)S(1)}, u32[]{:S(2)}, u32[]{:S(2)}) collective-permute-start(bf16[48,2048]{1,0:T(8,128)(2,1)S(1)} %copy-done.38), channel_id=1, source_target_pairs={{0,28},{4,24},{8,20},{12,16},{16,12},{20,8},{24,4},{28,0},{1,29},{... | collective-permute-start | bytes 589832 | tf_op jit(solution)/shard_map/ppermute | solution.py:93
  155.6 31.4 %collective-permute-start.21 = (bf16[48,2048]{1,0:T(8,128)(2,1)}, bf16[48,2048]{1,0:T(8,128)(2,1)S(1)}, u32[]{:S(2)}, u32[]{:S(2)}) collective-permute-start(bf16[48,2048]{1,0:T(8,128)(2,1)} %get-tuple-element.43), channel_id=1, source_target_pairs={{0,4},{4,0},{8,12},{12,8},{16,20},{20,16},{24,28},{28,24},{1,5},{5... | collective-permute-start | bytes 589832 | tf_op jit(solution)/shard_map/ppermute | solution.py:93
  156.9 30.8 %collective-permute-start.22 = (bf16[48,2048]{1,0:T(8,128)(2,1)}, bf16[48,2048]{1,0:T(8,128)(2,1)S(1)}, u32[]{:S(2)}, u32[]{:S(2)}) collective-permute-start(bf16[48,2048]{1,0:T(8,128)(2,1)} %get-tuple-element.44), channel_id=1, source_target_pairs={{0,8},{4,12},{8,0},{12,4},{16,24},{20,28},{24,16},{28,20},{1,9},{5... | collective-permute-start | bytes 589832 | tf_op jit(solution)/shard_map/ppermute | solution.py:93
  171.3 27.6 %collective-permute-start.23 = (bf16[48,2048]{1,0:T(8,128)(2,1)S(1)}, bf16[48,2048]{1,0:T(8,128)(2,1)S(1)}, u32[]{:S(2)}, u32[]{:S(2)}) collective-permute-start(bf16[48,2048]{1,0:T(8,128)(2,1)S(1)} %copy-done.45), channel_id=1, source_target_pairs={{0,12},{4,8},{8,4},{12,0},{16,28},{20,24},{24,20},{28,16},{1,13},{... | collective-permute-start | bytes 589832 | tf_op jit(solution)/shard_map/ppermute | solution.py:93
  176.6 22.2 %collective-permute-start.24 = (bf16[48,2048]{1,0:T(8,128)(2,1)S(1)}, bf16[48,2048]{1,0:T(8,128)(2,1)S(1)}, u32[]{:S(2)}, u32[]{:S(2)}) collective-permute-start(bf16[48,2048]{1,0:T(8,128)(2,1)S(1)} %copy-done.43), channel_id=1, source_target_pairs={{0,16},{4,20},{8,24},{12,28},{16,0},{20,4},{24,8},{28,12},{1,17},{... | collective-permute-start | bytes 589832 | tf_op jit(solution)/shard_map/ppermute | solution.py:93
  186.9 19.3 %collective-permute-start.25 = (bf16[48,2048]{1,0:T(8,128)(2,1)S(1)}, bf16[48,2048]{1,0:T(8,128)(2,1)S(1)}, u32[]{:S(2)}, u32[]{:S(2)}) collective-permute-start(bf16[48,2048]{1,0:T(8,128)(2,1)S(1)} %copy-done.42), channel_id=1, source_target_pairs={{0,20},{4,16},{8,28},{12,24},{16,4},{20,0},{24,12},{28,8},{1,21},{... | collective-permute-start | bytes 589832 | tf_op jit(solution)/shard_map/ppermute | solution.py:93
  186.9 24.7 %collective-permute-start.26 = (bf16[48,2048]{1,0:T(8,128)(2,1)S(1)}, bf16[48,2048]{1,0:T(8,128)(2,1)S(1)}, u32[]{:S(2)}, u32[]{:S(2)}) collective-permute-start(bf16[48,2048]{1,0:T(8,128)(2,1)S(1)} %copy-done.40), channel_id=1, source_target_pairs={{0,24},{4,28},{8,16},{12,20},{16,8},{20,12},{24,0},{28,4},{1,25},{... | collective-permute-start | bytes 589832 | tf_op jit(solution)/shard_map/ppermute | solution.py:93
  187.8 28.6 %collective-permute-start.27 = (bf16[48,2048]{1,0:T(8,128)(2,1)S(1)}, bf16[48,2048]{1,0:T(8,128)(2,1)S(1)}, u32[]{:S(2)}, u32[]{:S(2)}) collective-permute-start(bf16[48,2048]{1,0:T(8,128)(2,1)S(1)} %copy-done.39), channel_id=1, source_target_pairs={{0,28},{4,24},{8,20},{12,16},{16,12},{20,8},{24,4},{28,0},{1,29},{... | collective-permute-start | bytes 589832 | tf_op jit(solution)/shard_map/ppermute | solution.py:93
  (68 other events, 1192.1 us)
